TPU v7x, 32 devices: a whole 2x2x4 slice. The times are simulated.
32 devices in a mesh: sp: 8 (over z, y), tp: 4 (over x, core).
Axes of the slice: x: 2, y: 2, z: 4, core: 2. Of those that a mesh axis runs over, the one named last changes fastest.
Arguments:
- mixer_input: bfloat16 [1024, 1024], P('sp', 'tp'), may hold values from -1800 to 1800
- time_step: float32 [2, 64], P(None, 'tp'), may hold values from 0 to 2, as said below
- damping: float32 [2, 1024, 64], P(None, 'sp', 'tp'), may hold values from 0 to 2
- input_map: bfloat16 [2, 2, 64, 64, 16], P(None, None, 'tp'), may hold values from -1 to 1
- readout: float32 [2, 2, 64, 16, 64], P(None, None, 'tp'), may hold values from -0.5 to 0.5
- skip_gain: float32 [1024], P('tp'), may hold values from -4 to 4
- out_gain: float32 [1024], P('tp'), may hold values from 0.1 to 1.9
- out_weight: bfloat16 [1024, 2048], replicated, may hold values from -0.1875 to 0.1875
- residual: bfloat16 [1024, 2048], P(('sp', 'tp')), may hold values from -6 to 6
- channel_gain: float32 [2048], replicated, may hold values from 0.1 to 1.9
- value_weight: bfloat16 [2048, 6144], P('sp', 'tp'), may hold values from -0.125 to 0.125
- gate_weight: bfloat16 [2048, 6144], P('sp', 'tp'), may hold values from -0.125 to 0.125
- value_taps: float32 [3, 6144], P(None, 'tp'), may hold values from -3 to 3
- gate_taps: float32 [3, 6144], P(None, 'tp'), may hold values from -3 to 3
- down_weight: bfloat16 [6144, 2048], P('tp', 'sp'), may hold values from -0.078125 to 0.078125
Outputs:
- output: bfloat16 [1024, 2048], P(('sp', 'tp'))
Inputs may be any that keep to these rules, and one draw needn't show every extreme that they name: `time_step`: positive.
All inputs are finite; a program needn't handle non-finite values.
Results may differ from a plain program's by a relative error of at most 0.017.
Values may be sent and summed in bfloat16 or wider, within the bound.
A program may use at most 128 MiB of HBM per device.

v0:
```python
import math

import jax
import jax.numpy as jnp
from jax import lax
from jax.experimental import pallas as pl
from jax.experimental.pallas import tpu as pltpu
from jax.sharding import PartitionSpec as P

norm_eps = 1e-06
highest = lax.Precision.HIGHEST
mesh_ids = pl.DeviceIdType.MESH


def carry_kernel(count, own_ref, all_ref, local_sem, send_sem, recv_sem):
    sp, tp = lax.axis_index("sp"), lax.axis_index("tp")
    barrier = pltpu.get_barrier_semaphore()
    for offset in range(1, count):
        peer = lax.rem(sp + offset, count)
        pl.semaphore_signal(barrier, inc=1, device_id=(peer, tp), device_id_type=mesh_ids)
    pl.semaphore_wait(barrier, count - 1)
    keep = pltpu.make_async_copy(own_ref, all_ref.at[sp], local_sem)
    keep.start()
    copies = []
    for offset in range(1, count):
        peer = lax.rem(sp + offset, count)
        copy = pltpu.make_async_remote_copy(
            src_ref=own_ref,
            dst_ref=all_ref.at[sp],
            send_sem=send_sem.at[offset],
            recv_sem=recv_sem.at[offset],
            device_id=(peer, tp),
            device_id_type=mesh_ids,
        )
        copy.start()
        copies.append(copy)
    keep.wait()
    for copy in copies:
        copy.wait()


def gather_ends(packed, count):
    vmem = pl.BlockSpec(memory_space=pltpu.VMEM)
    return pl.pallas_call(
        lambda *refs: carry_kernel(count, *refs),
        name="gather_ends",
        out_shape=jax.ShapeDtypeStruct((count,) + packed.shape, packed.dtype),
        in_specs=[vmem],
        out_specs=vmem,
        scratch_shapes=[
            pltpu.SemaphoreType.DMA,
            pltpu.SemaphoreType.DMA((count,)),
            pltpu.SemaphoreType.DMA((count,)),
        ],
        compiler_params=pltpu.CompilerParams(collective_id=0, has_side_effects=True),
    )(packed)


gather_orders = (("z", "y", "x", "c"), ("y", "z", "x", "c"))
sum_orders = (("c", "x", "y", "z"), ("c", "z", "y", "x"))
axes = ("z", "y", "x", "c")


def channel_kernel(sizes, *refs):
    normed_ref, hidden_state_ref, up_send, down_send, taps_ref, out_ref = refs[:6]
    rows_all, up_rows, partial, up_land, down_land, down_ref = refs[6:12]
    landing = refs[12:20]
    local_sem, send_sem, recv_sem, weight_send_sem, weight_recv_sem = refs[20:25]
    rows, width = normed_ref.shape
    half = width // 2
    count, part, part_width = down_send.shape
    sp, tp = lax.axis_index("sp"), lax.axis_index("tp")
    mine = {
        "z": sp // sizes["y"],
        "y": lax.rem(sp, sizes["y"]),
        "x": tp // sizes["c"],
        "c": lax.rem(tp, sizes["c"]),
    }

    def neighbour(axis, offset):
        at = dict(mine)
        at[axis] = lax.rem(mine[axis] + offset, sizes[axis])
        return at[axis], (at["z"] * sizes["y"] + at["y"], at["x"] * sizes["c"] + at["c"])

    barrier = pltpu.get_barrier_semaphore()
    greeted = 0
    for axis in ("x", "c"):
        for offset in range(1, sizes[axis]):
            _, device = neighbour(axis, offset)
            pl.semaphore_signal(barrier, inc=1, device_id=device, device_id_type=mesh_ids)
            greeted += 1
    for offset in range(1, count):
        peer = lax.rem(sp + offset, count)
        pl.semaphore_signal(barrier, inc=1, device_id=(peer, tp), device_id_type=mesh_ids)
        greeted += 1
    pl.semaphore_wait(barrier, greeted)

    keeps = []
    for kind, (source, target) in enumerate(
        (
            (normed_ref, rows_all.at[mine["z"], mine["y"], mine["x"], mine["c"]]),
            (up_send.at[sp], up_land.at[sp]),
            (down_send.at[sp], down_land.at[sp]),
        )
    ):
        keep = pltpu.make_async_copy(source, target, local_sem.at[kind])
        keep.start()
        keeps.append(keep)
    keeps[0].wait()

    def spread(source, land, kind):
        started = []
        for offset in range(1, count):
            peer = lax.rem(sp + offset, count)
            copy = pltpu.make_async_remote_copy(
                src_ref=source.at[peer],
                dst_ref=land.at[sp],
                send_sem=weight_send_sem.at[kind, offset],
                recv_sem=weight_recv_sem.at[kind, offset],
                device_id=(peer, tp),
                device_id_type=mesh_ids,
            )
            copy.start()
            started.append(copy)
        return started

    slot = 0
    pending = [[], []]
    up_copies, down_copies = [], []
    for stage in range(4):
        if stage == 2:
            up_copies = spread(up_send, up_land, 0)
            down_copies = spread(down_send, down_land, 1)
        for piece in range(2):
            axis = gather_orders[piece][stage]
            done = gather_orders[piece][:stage]
            for copy in pending[piece]:
                copy.wait()
            pending[piece] = []
            index = tuple(slice(None) if name in done else mine[name] for name in axes)
            block = rows_all.at[index + (slice(None), pl.ds(piece * half, half))]
            for offset in range(1, sizes[axis]):
                _, device = neighbour(axis, offset)
                copy = pltpu.make_async_remote_copy(
                    src_ref=block,
                    dst_ref=block,
                    send_sem=send_sem.at[slot],
                    recv_sem=recv_sem.at[slot],
                    device_id=device,
                    device_id_type=mesh_ids,
                )
                copy.start()
                pending[piece].append(copy)
                slot += 1
    for piece in range(2):
        for copy in pending[piece]:
            copy.wait()

    plane = sizes["y"] * sizes["x"] * sizes["c"] * rows
    total = plane * sizes["z"]
    for copy in [keeps[1]] + up_copies:
        copy.wait()
    edge = jnp.zeros((8, up_rows.shape[1]), jnp.float32)
    up_rows[pl.ds(0, 8), :] = edge
    up_rows[pl.ds(total + 8, 8), :] = edge

    def project(z, _):
        block = rows_all[z].reshape(plane, width)
        up_weight = up_land[...].reshape(width, 2 * part)
        up = jnp.dot(block, up_weight, preferred_element_type=jnp.float32)
        start = pl.multiple_of(z * plane + 8, 8)
        up_rows[pl.ds(start, plane), :] = up.astype(jnp.bfloat16).astype(jnp.float32)
        return _

    lax.fori_loop(0, sizes["z"], project, 0)

    for copy in [keeps[2]] + down_copies:
        copy.wait()
    for source in range(count):
        down_ref[:, source * part_width : (source + 1) * part_width] = down_land[source]

    def mix(z, _):
        start = pl.multiple_of(z * plane, 8)
        window = up_rows[pl.ds(start, plane + 16), :]
        convolved = (
            taps_ref[0:1, :] * window[7 : plane + 7]
            + taps_ref[1:2, :] * window[8 : plane + 8]
            + taps_ref[2:3, :] * window[9 : plane + 9]
        )
        gate = convolved[:, part:]
        hidden = convolved[:, :part] * (gate / (1.0 + jnp.exp(-gate)))
        sums = jnp.dot(
            hidden.astype(jnp.bfloat16), down_ref[...], preferred_element_type=jnp.float32
        )
        partial[z] = sums.astype(jnp.bfloat16).reshape(partial.shape[1:])
        return _

    lax.fori_loop(0, sizes["z"], mix, 0)

    def start_sum(piece, stage, slot):
        axis = sum_orders[piece][stage]
        done = sum_orders[piece][:stage]
        started = []
        for offset in range(1, sizes[axis]):
            place, device = neighbour(axis, offset)
            index = tuple(
                place if name == axis else mine[name] if name in done else slice(None)
                for name in axes
            )
            copy = pltpu.make_async_remote_copy(
                src_ref=partial.at[index + (slice(None), pl.ds(piece * half, half))],
                dst_ref=landing[piece * 4 + stage].at[offset - 1],
                send_sem=send_sem.at[slot],
                recv_sem=recv_sem.at[slot],
                device_id=device,
                device_id_type=mesh_ids,
            )
            copy.start()
            started.append(copy)
            slot += 1
        return started, slot

    def add_landed(piece, stage):
        axis = sum_orders[piece][stage]
        done = sum_orders[piece][: stage + 1]
        land = landing[piece * 4 + stage]
        columns = pl.ds(piece * half, half)
        free = [name for name in axes if name not in done]

        def add(step, _):
            index, inner = [], ()
            for name in axes:
                if name in done:
                    index.append(mine[name])
                elif name == free[0]:
                    index.append(step)
                    inner = (step,)
                else:
                    index.append(slice(None))
            index = tuple(index) + (slice(None), columns)
            value = partial[index].astype(jnp.float32)
            for offset in range(1, sizes[axis]):
                value = value + land[(offset - 1,) + inner].astype(jnp.float32)
            if free:
                partial[index] = value.astype(jnp.bfloat16)
            else:
                out_ref[:, columns] = (
                    hidden_state_ref[:, columns].astype(jnp.float32) + value
                ).astype(jnp.bfloat16)
            return _

        if free:
            lax.fori_loop(0, sizes[free[0]], add, 0)
        else:
            add(0, 0)

    slot = send_sem.shape[0] // 2
    for stage in range(4):
        for piece in range(2):
            if stage:
                for copy in pending[piece]:
                    copy.wait()
                add_landed(piece, stage - 1)
            pending[piece], slot = start_sum(piece, stage, slot)
    for piece in range(2):
        for copy in pending[piece]:
            copy.wait()
        add_landed(piece, 3)


def channel_mixer(normed, hidden_state, up_send, down_send, taps, sp_count, tp_count):
    cores = 2
    across = tp_count // cores
    deep = math.gcd(across, sp_count)
    sizes = {"z": sp_count // deep, "y": deep, "x": across, "c": cores}
    rows, width = normed.shape
    half = width // 2
    grid = tuple(sizes[name] for name in axes)
    total = math.prod(grid) * rows
    landing = []
    for order in sum_orders:
        for stage in range(4):
            axis = order[stage]
            left = tuple(sizes[name] for name in axes if name not in order[: stage + 1])
            landing.append(
                pltpu.VMEM((max(sizes[axis] - 1, 1),) + left + (rows, half), jnp.bfloat16)
            )
    copies = 2 * 2 * sum(max(sizes[name] - 1, 0) for name in axes)
    vmem = pl.BlockSpec(memory_space=pltpu.VMEM)
    return pl.pallas_call(
        lambda *refs: channel_kernel(sizes, *refs),
        name="channel_mixer",
        out_shape=jax.ShapeDtypeStruct((rows, width), jnp.bfloat16),
        in_specs=[vmem] * 5,
        out_specs=vmem,
        scratch_shapes=[
            pltpu.VMEM(grid + (rows, width), jnp.bfloat16),
            pltpu.VMEM((total + 16, up_send.shape[2]), jnp.float32),
            pltpu.VMEM(grid + (rows, width), jnp.bfloat16),
            pltpu.VMEM(up_send.shape, jnp.bfloat16),
            pltpu.VMEM(down_send.shape, jnp.bfloat16),
            pltpu.VMEM((down_send.shape[1], width), jnp.bfloat16),
            *landing,
            pltpu.SemaphoreType.DMA((3,)),
            pltpu.SemaphoreType.DMA((copies,)),
            pltpu.SemaphoreType.DMA((copies,)),
            pltpu.SemaphoreType.DMA((2, sp_count)),
            pltpu.SemaphoreType.DMA((2, sp_count)),
        ],
        compiler_params=pltpu.CompilerParams(
            collective_id=1, has_side_effects=True, vmem_limit_bytes=63 * 1024 * 1024
        ),
    )(normed, hidden_state, up_send, down_send, taps)


def turns(step_size, count):
    coarse = jnp.round(step_size * 1024.0) / 1024.0
    whole = coarse * count
    whole = whole - 2.0 * jnp.floor(whole * 0.5)
    return whole + (step_size - coarse) * count


def mixer(mixer_input, time_step, damping, input_map, readout, skip_gain):
    rows = mixer_input.shape[0]
    groups = time_step.shape[1]
    states, width = input_map.shape[3], input_map.shape[4]
    count, mine = lax.axis_size("sp"), lax.axis_index("sp")
    at = jnp.arange(rows)
    lower = at[:, None] >= at[None, :]
    reach = jnp.stack((lower, lower.T))
    log_decay = -0.5 * time_step[:, None, :] - damping
    log_sum = jnp.einsum("ktu,kug->kgt", reach.astype(jnp.float32), log_decay, precision=highest)
    weights = jnp.where(
        reach[:, None],
        jnp.exp(jnp.minimum(log_sum[:, :, :, None] - log_sum[:, :, None, :], 0.0)),
        0.0,
    )
    number = jnp.arange(states, dtype=jnp.float32)
    dt = time_step[:, :, None, None]
    angle = math.pi * turns(dt, number[None, :] * at.astype(jnp.float32)[:, None])
    sign = jnp.array([1.0, -1.0], jnp.float32)[:, None, None, None]
    cos, sin = jnp.cos(angle), jnp.sin(angle) * sign
    grouped = mixer_input.reshape(rows, groups, width)
    drive = jnp.einsum("tgh,kpgnh->kpgtn", grouped, input_map, preferred_element_type=jnp.float32)
    drive = drive * jnp.sqrt(-jnp.expm1(-time_step))[:, None, :, None, None]
    rotated = jnp.concatenate(
        (cos * drive[:, 0] + sin * drive[:, 1], cos * drive[:, 1] - sin * drive[:, 0]), axis=3
    )
    local = jnp.einsum("kgts,kgsn->kgtn", weights, rotated, precision=lax.Precision.HIGH)
    ends = jnp.stack((local[0, :, -1], local[1, :, 0]))
    totals = jnp.stack((log_sum[0, :, -1], log_sum[1, :, 0]))
    flat = ends.reshape(2 * groups, 2 * states)
    spare = jnp.pad(totals.reshape(1, 2 * groups), ((0, 7), (0, 2 * states - 2 * groups)))
    every = gather_ends(jnp.concatenate((flat, spare), axis=0), count)
    end_all = every[:, : 2 * groups].reshape(count, 2, groups, 2 * states)
    total_all = every[:, 2 * groups, : 2 * groups].reshape(count, 2, groups)
    index = jnp.arange(count)
    away = jnp.stack((mine - index, index - mine), axis=1)
    lo = jnp.minimum(index, mine)[:, None]
    hi = jnp.maximum(index, mine)[:, None]
    between = ((index[None, :] > lo) & (index[None, :] < hi)).astype(jnp.float32)
    span = jnp.einsum("ji,ikg->jkg", between, total_all, precision=highest)
    factor = jnp.where(away[:, :, None] > 0, jnp.exp(span), 0.0)
    block_turn = turns(time_step[:, :, None], number * rows)
    hop = jnp.abs(mine - index).astype(jnp.float32)[:, None, None, None] * block_turn
    hop = math.pi * (hop - 2.0 * jnp.floor(hop * 0.5))
    hop_cos, hop_sin = jnp.cos(hop) * factor[..., None], jnp.sin(hop) * factor[..., None]
    end_re, end_im = end_all[..., :states], end_all[..., states:]
    carry = jnp.concatenate(
        (
            jnp.sum(hop_cos * end_re - hop_sin * end_im, axis=0),
            jnp.sum(hop_cos * end_im + hop_sin * end_re, axis=0),
        ),
        axis=2,
    )
    local = local + jnp.exp(log_sum)[..., None] * carry[:, :, None, :]
    re, im = local[..., :states], local[..., states:]
    state = jnp.concatenate((cos * re - sin * im, cos * im + sin * re), axis=3)
    out_map = jnp.concatenate((readout[:, 0], -readout[:, 1]), axis=3)
    mixed = jnp.einsum("kgtn,kghn->tgh", state, out_map, precision=lax.Precision.HIGH)
    return mixed.reshape(rows, groups * width) + skip_gain[None, :] * mixer_input.astype(
        jnp.float32
    )


def body(
    mixer_input,
    time_step,
    damping,
    input_map,
    readout,
    skip_gain,
    out_gain,
    out_weight,
    residual,
    channel_gain,
    value_weight,
    gate_weight,
    value_taps,
    gate_taps,
    down_weight,
):
    count, mine = lax.axis_size("sp"), lax.axis_index("sp")
    depth, hidden_width = value_weight.shape
    part = hidden_width // count
    up_send = jnp.concatenate(
        (
            value_weight.reshape(depth, count, part).swapaxes(0, 1),
            gate_weight.reshape(depth, count, part).swapaxes(0, 1),
        ),
        axis=2,
    )
    down_send = down_weight.reshape(count, part, down_weight.shape[1])
    mixed_y = mixer(mixer_input, time_step, damping, input_map, readout, skip_gain)
    tp_count = lax.axis_size("tp")
    mixed_y = mixed_y.reshape(tp_count, -1, out_gain.shape[0])
    gain_row = jnp.broadcast_to(out_gain, (tp_count, 1, out_gain.shape[0]))
    mixed_y = jnp.concatenate((mixed_y, gain_row), axis=1)
    mixed_y = lax.all_to_all(mixed_y, "tp", split_axis=0, concat_axis=0, tiled=True)
    mixed_y = mixed_y.swapaxes(0, 1).reshape(mixed_y.shape[1], -1)
    mixed_y, gain = mixed_y[:-1], mixed_y[-1]
    inverse = lax.rsqrt(jnp.mean(mixed_y * mixed_y, axis=1, keepdims=True) + norm_eps)
    normed_mix = (mixed_y * inverse * gain[None, :]).astype(jnp.bfloat16)
    mixed_rows = jnp.dot(normed_mix, out_weight, preferred_element_type=jnp.float32)
    hidden_state = (residual.astype(jnp.float32) + mixed_rows).astype(jnp.bfloat16)
    state_wide = hidden_state.astype(jnp.float32)
    scale_rows = lax.rsqrt(jnp.mean(state_wide * state_wide, axis=1, keepdims=True) + norm_eps)
    normed = (state_wide * scale_rows * channel_gain[None, :]).astype(jnp.bfloat16)
    taps = jnp.concatenate(
        (
            lax.dynamic_slice_in_dim(value_taps, mine * part, part, axis=1),
            lax.dynamic_slice_in_dim(gate_taps, mine * part, part, axis=1),
        ),
        axis=1,
    )
    return channel_mixer(normed, hidden_state, up_send, down_send, taps, count, tp_count)


def solution(mesh):
    in_specs = (
        P("sp", "tp"),
        P(None, "tp"),
        P(None, "sp", "tp"),
        P(None, None, "tp", None, None),
        P(None, None, "tp", None, None),
        P("tp"),
        P("tp"),
        P(),
        P(("sp", "tp"), None),
        P(),
        P("sp", "tp"),
        P("sp", "tp"),
        P(None, "tp"),
        P(None, "tp"),
        P("tp", "sp"),
    )
    out_specs = P(("sp", "tp"), None)
    return jax.shard_map(body, mesh=mesh, in_specs=in_specs, out_specs=out_specs, check_vma=False)
```

profile of v0, /device:TPU:0, one launch (start us, length us, event | category | flops | bytes accessed | tf_op | source)
XLA Modules:
  0.0 168.0 jit_solution(2502206506006835890)
XLA Ops:
  0.1 0.7 broadcast_multiply_fusion
  1.0 1.0 copy.58
  2.0 1.0 fusion.55
  3.2 1.5 bitcast_multiply_fusion
  4.7 4.5 %multiply_add_fusion.2 = (f32[2,16,128,64]{2,3,0,1:T(8,128)S(1)}, f32[2,16,128,64]{2,3,0,1:T(8,128)S(1)}) fusion(f32[2,2,16,128,64]{3,4,1,0,2:T(8,128)S(1)} %bitcast_multiply_fusion, f32[2]{0:T(128)S(1)} %copy-done.7, f32[2,16]{0,1:T(8,128)S(1)} %copy.57, f32[128,64]{0,1:T(8,128)S(1)} %iota_multiply_fusion, f32[2,16]{0,1:T(8,128)S(1)} %copy.56), kind=kLoop, calls=%fused_computation.29 | loop fusion | flops 3932160 | bytes 4227336 | tf_op jit(solution)/shard_map/add | solution.py:347
  9.2 2.4 %fusion.5 = f32[2,16,128,128]{3,2,1,0:T(8,128)S(1)} fusion(f32[2,16,128]{2,1,0:T(8,128)S(1)} %get-tuple-element.24, pred[2,128,128]{2,1,0:T(8,128)(4,1)S(1)} %pad_add_fusion, f32[2,16,128,64]{2,3,0,1:T(8,128)S(1)} %get-tuple-element.12, f32[2,16,128,64]{2,3,0,1:T(8,128)S(1)} %get-tuple-element.11), kind=kOutput, calls=%fused_computation.7 | convolution fusion | flops 404750336 | bytes 4243456 | tf_op jit(solution)/shard_map/kgts,kgsn->kgtn/dot_general | solution.py:349
  11.6 1.3 copy-done
  13.7 11.0 %gather_ends.1 = f32[8,40,128]{2,1,0:T(8,128)} custom-call(f32[40,128]{1,0:T(8,128)} %select_maximum_fusion.refs_0_), custom_call_target="tpu_custom_call" | custom-call | tf_op jit(solution)/shard_map/gather_ends/pallas_call | solution.py:44
  24.7 0.8 slice_reduce_fusion.2
  25.5 2.0 %copy.68 = f32[2,16,128,128]{2,3,0,1:T(8,128)S(1)} copy(f32[2,16,128,128]{3,2,1,0:T(8,128)} %copy-done) | data formatting | bytes 4194304 | tf_op jit(solution)/shard_map/kgts,kgsn->kgtn/dot_general | solution.py:349
  27.9 0.6 subtract_reduce_fusion
  28.6 0.7 multiply_add_fusion
  29.4 4.5 %multiply_subtract_fusion.1 = (f32[2,16,128,64]{2,3,0,1:T(8,128)S(1)}, f32[2,16,128,64]{2,3,0,1:T(8,128)S(1)}) fusion(f32[2,16,128,128]{2,3,0,1:T(8,128)S(1)} %multiply_add_fusion, f32[2]{0:T(128)S(1)} %copy-done.7, f32[2,16]{0,1:T(8,128)S(1)} %copy.57, f32[128,64]{0,1:T(8,128)S(1)} %iota_multiply_fusion, f32[2,16]{0,1:T(8,128)S(1)} %copy.56), kind=kLoop, calls=%fused_computation.27 | loop fusion | flops 3932160 | bytes 4227336 | tf_op jit(solution)/shard_map/sub | solution.py:378
  34.0 0.8 fusion.1
  35.0 0.7 pad_maximum_fusion.2
  35.7 3.3 %all-to-all-start = ((f32[4,33,256]{2,1,0:T(8,128)}), f32[4,33,256]{2,1,0:T(8,128)S(1)}, u32[]{:S(2)}, u32[]{:S(2)}) async-start(f32[4,33,256]{2,1,0:T(8,128)} %pad_maximum_fusion.2), calls=%async_computation | async-start | bytes 327680 | tf_op jit(solution)/shard_map/all_to_all | solution.py:419
  39.8 1.4 copy.74
  41.8 1.7 %pad_maximum_fusion.1.refs_2_ = bf16[8,256,384]{2,1,0:T(8,128)(2,1)} fusion(bf16[8,256,192]{2,1,0:T(8,128)(2,1)S(1)} %bitcast.56, bf16[8,256,192]{2,1,0:T(8,128)(2,1)S(1)} %bitcast.55), kind=kLoop, calls=%fused_computation.15 | loop fusion | flops 3145728 | bytes 3145728 | tf_op jit(solution)/shard_map/concatenate | solution.py:406
  43.5 0.8 constant_dynamic-slice_fusion
  44.3 0.7 pad_maximum_fusion.5.refs_4_
  45.1 3.2 %fusion.21 = (f32[32]{0:T(128)S(1)}, bf16[32,2048]{1,0:T(8,128)(2,1)S(1)}) fusion(bf16[1024,2048]{1,0:T(8,128)(2,1)} %param.23, f32[32,1024]{1,0:T(8,128)S(1)} %bitcast.63, f32[1024]{0:T(1024)S(1)} %bitcast.70, f32[32]{0:T(128)S(1)} %add_rsqrt_fusion.1, bf16[32,2048]{1,0:T(8,128)(2,1)S(1)} %copy-done.5), kind=kOutput, calls=%fused_computation.38 | convolution fusion | flops 134709216 | bytes 4591872 | tf_op jit(solution)/shard_map/dot_general | solution.py:424
  48.3 0.8 fusion.23.refs_0_
  49.1 117.3 %channel_mixer.1 = bf16[32,2048]{1,0:T(8,128)(2,1)} custom-call(bf16[32,2048]{1,0:T(8,128)(2,1)} %fusion.23.refs_0_, bf16[32,2048]{1,0:T(8,128)(2,1)} %copy-done.1, bf16[8,256,384]{2,1,0:T(8,128)(2,1)} %pad_maximum_fusion.1.refs_2_, bf16[8,192,256]{2,1,0:T(8,128)(2,1)} %bitcast.60, f32[3,384]{1,0:T(4,128)} %pad_maximum_fusion.5.refs_4_), custom_call_target="tpu_custom_call" | custom-call | tf_op jit(solution)/shard_map/channel_mixer/pallas_call | solution.py:290
  166.4 1.6 copy.103
  (60 shorter events, 3.4 us)
Async XLA Ops:
  0.0 4.7 %copy-start.7 = (f32[2]{0:T(128)S(1)}, f32[2]{0:T(128)}, u32[]{:S(2)}) copy-start(f32[2]{0:T(128)} %constant.15.clone) | copy-start | bytes 28
  11.6 1.3 copy-start
  25.5 2.4 %slice-start = ((f32[8,40,128]{2,1,0:T(8,128)}), f32[8,32,128]{2,1,0:T(8,128)S(1)}, s32[]{:S(2)}) async-start(f32[8,40,128]{2,1,0:T(8,128)} %gather_ends.1), calls=%async_computation.1 | async-start | bytes 262144 | tf_op jit(solution)/shard_map/slice | solution.py:355
  29.3 4.5 %copy-start.3 = (f32[2,2,16,16,64]{4,3,2,1,0:T(8,128)S(1)}, f32[2,2,16,16,64]{4,3,2,1,0:T(8,128)}, u32[]{:S(2)}) copy-start(f32[2,2,16,16,64]{4,3,2,1,0:T(8,128)} %param.20) | copy-start | bytes 786436
  33.9 1.0 copy-start.4
  33.9 1.0 copy-start.8
  33.9 1.0 copy-start.9
  34.0 5.0 %copy-start.2 = (bf16[256,1536]{1,0:T(8,128)(2,1)S(1)}, bf16[256,1536]{1,0:T(8,128)(2,1)}, u32[]{:S(2)}) copy-start(bf16[256,1536]{1,0:T(8,128)(2,1)} %param.26) | copy-start | bytes 2359300
  35.7 9.3 %all-to-all-start = ((f32[4,33,256]{2,1,0:T(8,128)}), f32[4,33,256]{2,1,0:T(8,128)S(1)}, u32[]{:S(2)}, u32[]{:S(2)}) async-start(f32[4,33,256]{2,1,0:T(8,128)} %pad_maximum_fusion.2), calls=%async_computation | async-start | bytes 327680 | tf_op jit(solution)/shard_map/all_to_all | solution.py:419
  41.7 3.3 %copy-start.5 = (bf16[32,2048]{1,0:T(8,128)(2,1)S(1)}, bf16[32,2048]{1,0:T(8,128)(2,1)}, u32[]{:S(2)}) copy-start(bf16[32,2048]{1,0:T(8,128)(2,1)} %param.24) | copy-start | bytes 393220
  45.1 3.2 %copy-start.6 = (f32[2048]{0:T(1024)S(1)}, f32[2048]{0:T(1024)}, u32[]{:S(2)}) copy-start(f32[2048]{0:T(1024)} %param.25) | copy-start | bytes 24580
  48.3 0.8 copy-start.1
where the time goes:
time: 169 us; the launch traced here: 168 us
  Pallas kernels  128 us (76%)
  other arithmetic  15.9 us (9%)
  local copies, waits for them, and re-layouts  10.9 us (6%)
  matrix products  9.03 us (5%)
  starting transfers between devices  3.34 us (2%)
    pallas_call x1, Pallas kernels, channel_mixer(): pl.pallas_call(lambda *refs: channel_kernel(sizes, *refs), name='channel_...  117 us
    pallas_call x1, Pallas kernels, gather_ends(): pl.pallas_call(lambda *refs: carry_kernel(count, *refs), name='gather_end...  11 us
    unnamed x24, local copies, waits for them, and re-layouts  5.59 us
    add x1, other arithmetic, mixer(): cos * drive[:, 0] + sin * drive[:, 1]  4.5 us
    sub x1, other arithmetic, mixer(): state = jnp.concatenate((cos * re - sin * im, cos * im + sin * re), axis=3)  4.5 us
  transfers between devices with their start and end apart: 1, of which 0 were waited for; matrix products, arithmetic and copies ran while one was open for 3% of the time, Pallas kernels for 0%

commit v1 on v0

--- a/solution.py
+++ b/solution.py
@@ -383,6 +383,708 @@
     )
 
 
+gather_paths = (("z", "y", "x"), ("z", "x", "y")) * 2
+sum_paths = (("x", "y", "z"), ("y", "x", "z")) * 2
+chip_axes = ("z", "y", "x")
+
+
+def layer_kernel(sizes, *refs):
+    (
+        x_ref,
+        step_ref,
+        damping_ref,
+        tab_ref,
+        turn_ref,
+        in_ref,
+        readout_ref,
+        vec_ref,
+        taps_ref,
+        residual_ref,
+        channel_ref,
+        out_w_hbm,
+        value_hbm,
+        gate_hbm,
+        down_hbm,
+        out_ref,
+        x_t,
+        decay_parts,
+        local,
+        carried,
+        packet,
+        packets,
+        carry,
+        y_all,
+        y_land,
+        vec_all,
+        out_w,
+        state_rows,
+        taps,
+        up_w,
+        down_w,
+        rows_all,
+        up_rows,
+        hidden_rows,
+        partial,
+    ) = refs[:35]
+    pieces = len(gather_paths)
+    landing = refs[35 : 35 + 3 * pieces]
+    (
+        local_sem,
+        small_send,
+        small_recv,
+        taps_sem,
+        hop_send,
+        hop_recv,
+        w_send,
+        w_recv,
+        f_send,
+        f_recv,
+    ) = refs[35 + 3 * pieces :]
+    span, channels = x_ref.shape
+    pairs, heads, lanes = in_ref.shape[0], in_ref.shape[1], tab_ref.shape[3]
+    groups = step_ref.shape[1]
+    tiles = span // 8
+    rows, width = residual_ref.shape
+    piece_width = width // pieces
+    depth = value_hbm.shape[0]
+    part = down_hbm.shape[1]
+    unit = taps.shape[1]
+    cores = sizes["c"]
+    count, tp_count = sizes["z"] * sizes["y"], sizes["x"] * cores
+    per = count // cores
+    blocks = count * sizes["x"]
+    sp, tp = lax.axis_index("sp"), lax.axis_index("tp")
+    mine = {
+        "z": sp // sizes["y"],
+        "y": lax.rem(sp, sizes["y"]),
+        "x": tp // cores,
+        "c": lax.rem(tp, cores),
+    }
+    core = mine["c"]
+    partner = (sp, mine["x"] * cores + lax.rem(core + 1, cores))
+
+    def neighbour(axis, offset):
+        at = dict(mine)
+        at[axis] = lax.rem(mine[axis] + offset, sizes[axis])
+        return at[axis], (at["z"] * sizes["y"] + at["y"], at["x"] * cores + at["c"])
+
+    def remote(source, target, send, recv, device):
+        return pltpu.make_async_remote_copy(
+            src_ref=source,
+            dst_ref=target,
+            send_sem=send,
+            recv_sem=recv,
+            device_id=device,
+            device_id_type=mesh_ids,
+        )
+
+    barrier = pltpu.get_barrier_semaphore()
+    greeted = 0
+    for offset in range(count):
+        for turn in range(cores):
+            if offset or turn:
+                peer = lax.rem(sp + offset, count)
+                other = mine["x"] * cores + lax.rem(core + turn, cores)
+                pl.semaphore_signal(barrier, inc=1, device_id=(peer, other), device_id_type=mesh_ids)
+                greeted += 1
+    for offset in range(1, sizes["x"]):
+        for turn in range(cores):
+            other = lax.rem(mine["x"] + offset, sizes["x"]) * cores + turn
+            pl.semaphore_signal(barrier, inc=1, device_id=(sp, other), device_id_type=mesh_ids)
+            greeted += 1
+
+    out_copy = pltpu.make_async_copy(out_w_hbm, out_w, local_sem.at[0])
+    out_copy.start()
+    pl.semaphore_wait(barrier, greeted)
+
+    def block_view(kind, source):
+        if kind == 2:
+            return down_w.at[:, pl.ds(pl.multiple_of(source * part, part), part)]
+        column = kind * unit
+        return up_w.at[pl.ds(pl.multiple_of(source * depth, depth), depth), pl.ds(column, unit)]
+
+    keeper = lax.rem(sp, cores)
+
+    def weight_copy(kind, slot):
+        place = lax.rem(slot + sp, per)
+        chip = core * per + place
+        start = pl.multiple_of(place * unit, unit)
+        if kind == 2:
+            source = down_hbm.at[pl.ds(start, unit), :]
+        else:
+            source = (value_hbm, gate_hbm)[kind].at[:, pl.ds(start, unit)]
+        stays = (chip == sp) & (keeper == core)
+        target = block_view(kind, sp)
+        device = (chip, mine["x"] * cores + keeper)
+
+        def here():
+            return pltpu.make_async_copy(source, target, w_recv.at[kind, sp])
+
+        def away():
+            return remote(source, target, w_send.at[kind, slot], w_recv.at[kind, sp], device)
+
+        return stays, here, away
+
+    def send_weights(kinds, slots):
+        for slot in slots:
+            for kind in kinds:
+                stays, here, away = weight_copy(kind, slot)
+                pl.when(stays)(lambda: here().start())
+                pl.when(jnp.logical_not(stays))(lambda: away().start())
+
+    def finish_sends():
+        for slot in range(per):
+            for kind in range(3):
+                stays, _, away = weight_copy(kind, slot)
+                pl.when(jnp.logical_not(stays))(lambda: away().wait_send())
+
+    def forward_weights(kinds):
+        started = []
+        for index in range(per):
+            for kind in kinds:
+                source = core + cores * index
+                view = block_view(kind, source)
+                remote(view, view, w_send.at[kind, 0], w_recv.at[kind, source], partner).wait_recv()
+                copy = remote(view, view, f_send.at[kind, index], f_recv.at[kind, index], partner)
+                copy.start()
+                started.append(copy)
+        return started
+
+    def forwarded(kinds, started):
+        for copy in started:
+            copy.wait_send()
+        for index in range(per):
+            for kind in kinds:
+                view = block_view(kind, lax.rem(core + 1, cores) + cores * index)
+                remote(view, view, f_send.at[kind, index], f_recv.at[kind, index], partner).wait_recv()
+
+    send_weights((0,), (0,))
+
+    vec_copies = []
+    for offset in range(1, tp_count):
+        copy = remote(
+            vec_ref,
+            vec_all.at[tp],
+            small_send.at[0, offset],
+            small_recv.at[0, offset],
+            (sp, lax.rem(tp + offset, tp_count)),
+        )
+        copy.start()
+        vec_copies.append(copy)
+    vec_all[tp] = vec_ref[...]
+
+    owns_taps = core == sp // per
+    taps_view = taps_ref.at[:, pl.ds(pl.multiple_of(lax.rem(sp, per) * unit, unit), unit)]
+    taps_keep = pltpu.make_async_copy(taps_view, taps, taps_sem.at[0])
+    taps_send = remote(taps_view, taps, taps_sem.at[1], taps_sem.at[2], partner)
+
+    @pl.when(owns_taps)
+    def _():
+        taps_keep.start()
+        taps_send.start()
+
+    x_t[...] = jnp.transpose(x_ref[...].astype(jnp.float32)).astype(jnp.bfloat16)
+    for k in range(2):
+        left = jnp.exp(-0.5 * step_ref[k : k + 1, :] - damping_ref[k])
+        for level in range(3):
+            rounded = left.astype(jnp.bfloat16)
+            decay_parts[k, :, level * groups : (level + 1) * groups] = rounded
+            left = left - rounded.astype(jnp.float32)
+
+    row_in_tile = lax.broadcasted_iota(jnp.int32, (1, 8, lanes), 1)
+    pick_row = lax.rem(lax.broadcasted_iota(jnp.int32, (3 * groups, lanes), 0), groups)
+    pick_lane = lax.broadcasted_iota(jnp.int32, (3 * groups, lanes), 1) // (lanes // 2)
+
+    def chain(k, at, start_real, start_imag):
+        real, imag = start_real, start_imag
+        found = [None] * tiles
+        for tile in range(tiles) if k == 0 else range(tiles - 1, -1, -1):
+            place = pl.ds(tile * 8, 8)
+            cos, sin = carried[at, 0, place, :], carried[at, 1, place, :]
+            full_real = local[at, 0, place, :] + (cos * real - sin * imag)
+            full_imag = local[at, 1, place, :] + (cos * imag + sin * real)
+            found[tile] = (full_real, full_imag)
+            edge = slice(7, 8) if k == 0 else slice(0, 1)
+            real = jnp.broadcast_to(full_real[edge], (8, lanes))
+            imag = jnp.broadcast_to(full_imag[edge], (8, lanes))
+        return found, real, imag
+
+    def first_pass(pair, _):
+        inputs = x_t[pl.ds(pl.multiple_of(pair * heads, heads), heads), :]
+        driven = lax.dot_general(
+            inputs, in_ref[pair], (((0,), (0,)), ((), ())), preferred_element_type=jnp.float32
+        )
+        for k in range(2):
+            at = k * pairs + pair
+            pick = (pick_row == 2 * pair + pick_lane).astype(jnp.bfloat16)
+            cover = jnp.dot(decay_parts[k], pick, preferred_element_type=jnp.float32)
+            cover = cover.reshape(tiles, 8, lanes)
+            base = 2 * k * lanes
+            scale = turn_ref[2, pl.ds(at, 1), :]
+            real = (driven[:, base : base + lanes] * scale).reshape(tiles, 8, lanes)
+            imag = (driven[:, base + lanes : base + 2 * lanes] * scale).reshape(tiles, 8, lanes)
+            for reach in (1, 2, 4):
+                row = reach - 1 if k == 0 else 8 - reach
+                shift = reach if k == 0 else 8 - reach
+                valid = row_in_tile >= reach if k == 0 else row_in_tile < 8 - reach
+                cos = tab_ref[at, 0, row : row + 1, :].reshape(1, 1, lanes)
+                sin = tab_ref[at, 1, row : row + 1, :].reshape(1, 1, lanes)
+                moved_real = pltpu.roll(real, shift, 1)
+                moved_imag = pltpu.roll(imag, shift, 1)
+                decay = jnp.where(valid, cover, 0.0)
+                real = real + decay * (cos * moved_real - sin * moved_imag)
+                imag = imag + decay * (cos * moved_imag + sin * moved_real)
+                cover = cover * jnp.where(valid, pltpu.roll(cover, shift, 1), 1.0)
+            local[at, 0] = real.reshape(span, lanes)
+            local[at, 1] = imag.reshape(span, lanes)
+            carried[at, 0] = (cover * tab_ref[at, 0].reshape(1, 8, lanes)).reshape(span, lanes)
+            carried[at, 1] = (cover * tab_ref[at, 1].reshape(1, 8, lanes)).reshape(span, lanes)
+        for k in range(2):
+            at = k * pairs + pair
+            none = jnp.zeros((8, lanes), jnp.float32)
+            real, imag = chain(k, at, none, none)[1:]
+            packet[pl.ds(at, 1), :] = real[0:1]
+            packet[pl.ds(2 * pairs + at, 1), :] = imag[0:1]
+        return _
+
+    packet[pl.ds(4 * pairs, 2 * pairs), :] = turn_ref[3]
+    lax.fori_loop(0, pairs, first_pass, 0)
+
+    packets[sp] = packet[...]
+    carry_copies = []
+    for offset in range(1, count):
+        copy = remote(
+            packet,
+            packets.at[sp],
+            small_send.at[1, offset],
+            small_recv.at[1, offset],
+            (lax.rem(sp + offset, count), tp),
+        )
+        copy.start()
+        carry_copies.append(copy)
+    send_weights((1,), (0,))
+    send_weights((0, 1), (1,))
+    for copy in carry_copies:
+        copy.wait()
+
+    for k in range(2):
+        at = pl.ds(k * pairs, pairs)
+        cos, sin = turn_ref[0, at, :], turn_ref[1, at, :]
+        real = jnp.zeros((pairs, lanes), jnp.float32)
+        imag = real
+        for index in range(count) if k == 0 else range(count - 1, -1, -1):
+            total = packets[index, pl.ds((4 + k) * pairs, pairs), :]
+            turned_real = cos * real - sin * imag
+            turned_imag = cos * imag + sin * real
+            before = (index < sp) if k == 0 else (index > sp)
+            real = jnp.where(before, packets[index, at, :] + total * turned_real, real)
+            imag = jnp.where(
+                before,
+                packets[index, pl.ds((2 + k) * pairs, pairs), :] + total * turned_imag,
+                imag,
+            )
+        carry[0, at, :] = real
+        carry[1, at, :] = imag
+
+    gains = vec_ref[1:2, :] * x_ref[...].astype(jnp.float32)
+    for pair in range(pairs):
+        parts = []
+        for k in range(2):
+            at = k * pairs + pair
+            real = jnp.broadcast_to(carry[0, at : at + 1, :], (8, lanes))
+            imag = jnp.broadcast_to(carry[1, at : at + 1, :], (8, lanes))
+            found, _, _ = chain(k, at, real, imag)
+            parts.append(jnp.concatenate([item[0] for item in found], axis=0))
+            parts.append(jnp.concatenate([item[1] for item in found], axis=0))
+        state = jnp.concatenate(parts, axis=1)
+        state_high = state.astype(jnp.bfloat16)
+        state_low = (state - state_high.astype(jnp.float32)).astype(jnp.bfloat16)
+        out_map = readout_ref[pair]
+        map_high = out_map.astype(jnp.bfloat16)
+        map_low = (out_map - map_high.astype(jnp.float32)).astype(jnp.bfloat16)
+
+        def apply(left, right):
+            return lax.dot_general(
+                left, right, (((1,), (1,)), ((), ())), preferred_element_type=jnp.float32
+            )
+
+        both = apply(state_high, jnp.concatenate((map_high, map_low), axis=0))
+        mixed = both[:, :heads] + both[:, heads:] + apply(state_low, map_high)
+        columns = slice(pair * heads, (pair + 1) * heads)
+        y_all[:, columns] = mixed + gains[:, columns]
+    y_copies = []
+    for offset in range(1, tp_count):
+        peer = lax.rem(tp + offset, tp_count)
+        copy = remote(
+            y_all.at[pl.ds(pl.multiple_of(peer * rows, rows), rows), :],
+            y_land.at[tp],
+            small_send.at[2, offset],
+            small_recv.at[2, offset],
+            (sp, peer),
+        )
+        copy.start()
+        y_copies.append(copy)
+    y_land[tp] = y_all[pl.ds(pl.multiple_of(tp * rows, rows), rows), :]
+    for copy in vec_copies + y_copies:
+        copy.wait()
+    out_copy.wait()
+
+    mixed = jnp.concatenate([y_land[peer] for peer in range(tp_count)], axis=1)
+    gain = jnp.concatenate([vec_all[peer, 0:1, :] for peer in range(tp_count)], axis=1)
+    inverse = lax.rsqrt(jnp.mean(mixed * mixed, axis=1, keepdims=True) + norm_eps)
+    normed_mix = (mixed * inverse * gain).astype(jnp.bfloat16)
+    square = jnp.zeros((rows, 1), jnp.float32)
+    tile = 512
+    for start in range(0, width, tile):
+        columns = pl.ds(start, tile)
+        mixed_rows = jnp.dot(normed_mix, out_w[:, columns], preferred_element_type=jnp.float32)
+        summed = (residual_ref[:, columns].astype(jnp.float32) + mixed_rows).astype(jnp.bfloat16)
+        state_rows[:, columns] = summed
+        wide = summed.astype(jnp.float32)
+        square = square + jnp.sum(wide * wide, axis=1, keepdims=True)
+    scale_rows = lax.rsqrt(square / width + norm_eps)
+    normed = state_rows[...].astype(jnp.float32) * scale_rows * channel_ref[...]
+    rows_all[mine["z"], mine["y"], mine["x"]] = normed.astype(jnp.bfloat16)
+
+    slot = 0
+    pending = [[] for _ in range(pieces)]
+    for stage in range(3):
+        for piece in range(pieces):
+            axis = gather_paths[piece][stage]
+            done = gather_paths[piece][:stage]
+            for copy in pending[piece]:
+                copy.wait()
+            pending[piece] = []
+            index = tuple(slice(None) if name in done else mine[name] for name in chip_axes)
+            block = rows_all.at[index + (slice(None), pl.ds(piece * piece_width, piece_width))]
+            for offset in range(1, sizes[axis]):
+                _, device = neighbour(axis, offset)
+                copy = remote(block, block, hop_send.at[slot], hop_recv.at[slot], device)
+                copy.start()
+                pending[piece].append(copy)
+                slot += 1
+        if stage == 0:
+            send_weights((0, 1), range(2, per))
+            send_weights((2,), range(per))
+    up_started = forward_weights((0, 1))
+    for piece in range(pieces):
+        for copy in pending[piece]:
+            copy.wait()
+    forwarded((0, 1), up_started)
+
+    @pl.when(core == 0)
+    def _():
+        up_rows[1, pl.ds(0, 8), :] = jnp.zeros((8, 2 * unit), jnp.float32)
+
+    @pl.when(core == cores - 1)
+    def _():
+        up_rows[blocks, pl.ds(rows + 8, 8), :] = jnp.zeros((8, 2 * unit), jnp.float32)
+
+    chunk = 256
+
+    def project(n, _):
+        columns = pl.ds(pl.multiple_of(n * chunk, chunk), chunk)
+        block = rows_all[...].reshape(blocks * rows, width)
+        up = jnp.dot(block, up_w[:, columns], preferred_element_type=jnp.float32)
+        up = up.astype(jnp.bfloat16).astype(jnp.float32)
+        up_rows[pl.ds(1, blocks), pl.ds(8, rows), columns] = up.reshape(blocks, rows, chunk)
+        return _
+
+    lax.fori_loop(0, 2 * unit // chunk, project, 0)
+
+    edges = []
+    for kind, (take, land, first) in enumerate(((rows, 0, 1 + core), (8, rows + 8, core))):
+        copy = remote(
+            up_rows.at[pl.ds(1, blocks), pl.ds(take, 8), :],
+            up_rows.at[pl.ds(first, blocks), pl.ds(land, 8), :],
+            small_send.at[3, kind],
+            small_recv.at[3, kind],
+            partner,
+        )
+        copy.start()
+        edges.append(copy)
+    down_started = forward_weights((2,))
+
+    @pl.when(owns_taps)
+    def _():
+        taps_keep.wait()
+        taps_send.wait_send()
+
+    @pl.when(jnp.logical_not(owns_taps))
+    def _():
+        taps_send.wait_recv()
+
+    for copy in edges:
+        copy.wait()
+
+    def mix(b, _):
+        window = up_rows[b + 1]
+
+        def conv(base, columns):
+            return (
+                taps[base : base + 1, :] * window[7 : rows + 7, columns]
+                + taps[base + 1 : base + 2, :] * window[8 : rows + 8, columns]
+                + taps[base + 2 : base + 3, :] * window[9 : rows + 9, columns]
+            )
+
+        value = conv(0, slice(0, unit))
+        gate = conv(3, slice(unit, 2 * unit))
+        hidden = value * (gate / (1.0 + jnp.exp(-gate)))
+        hidden_rows[pl.ds(pl.multiple_of(b * rows, rows), rows), :] = hidden.astype(jnp.bfloat16)
+        return _
+
+    lax.fori_loop(0, blocks, mix, 0)
+    forwarded((2,), down_started)
+
+    def start_sum(piece, stage, slot):
+        axis = sum_paths[piece][stage]
+        done = sum_paths[piece][:stage]
+        started = []
+        for offset in range(1, sizes[axis]):
+            place, device = neighbour(axis, offset)
+            index = tuple(
+                place if name == axis else mine[name] if name in done else slice(None)
+                for name in chip_axes
+            )
+            copy = remote(
+                partial.at[index + (slice(None), pl.ds(piece * piece_width, piece_width))],
+                landing[piece * 3 + stage].at[offset - 1],
+                hop_send.at[slot],
+                hop_recv.at[slot],
+                device,
+            )
+            copy.start()
+            started.append(copy)
+            slot += 1
+        return started, slot
+
+    def add_landed(piece, stage):
+        axis = sum_paths[piece][stage]
+        done = sum_paths[piece][: stage + 1]
+        land = landing[piece * 3 + stage]
+        columns = pl.ds(piece * piece_width, piece_width)
+        free = [name for name in chip_axes if name not in done]
+
+        def add(step, _):
+            index, inner = [], ()
+            for name in chip_axes:
+                if name in done:
+                    index.append(mine[name])
+                elif name == free[0]:
+                    index.append(step)
+                    inner = (step,)
+                else:
+                    index.append(slice(None))
+            index = tuple(index) + (slice(None), columns)
+            value = partial[index].astype(jnp.float32)
+            for offset in range(1, sizes[axis]):
+                value = value + land[(offset - 1,) + inner].astype(jnp.float32)
+            if free:
+                partial[index] = value.astype(jnp.bfloat16)
+            else:
+                out_ref[:, columns] = (
+                    state_rows[:, columns].astype(jnp.float32) + value
+                ).astype(jnp.bfloat16)
+            return _
+
+        if free:
+            lax.fori_loop(0, sizes[free[0]], add, 0)
+        else:
+            add(0, 0)
+
+    slot = hop_send.shape[0] // 2
+    pending = []
+    for piece in range(pieces):
+        columns = pl.ds(piece * piece_width, piece_width)
+        sums = jnp.dot(hidden_rows[...], down_w[:, columns], preferred_element_type=jnp.float32)
+        shape = partial.shape[:3] + (rows, piece_width)
+        partial[:, :, :, :, columns] = sums.astype(jnp.bfloat16).reshape(shape)
+        started, slot = start_sum(piece, 0, slot)
+        pending.append(started)
+    for stage in range(1, 3):
+        for piece in range(pieces):
+            for copy in pending[piece]:
+                copy.wait()
+            add_landed(piece, stage - 1)
+            pending[piece], slot = start_sum(piece, stage, slot)
+    for piece in range(pieces):
+        for copy in pending[piece]:
+            copy.wait()
+        add_landed(piece, 2)
+    finish_sends()
+
+
+def whole_layer(sizes, arrays, weights, unit):
+    x, time_step, _, tab, turn, in_map, _, vec, taps, residual, _ = arrays
+    out_weight, value_weight, gate_weight, down_weight = weights
+    span, channels = x.shape
+    groups, lanes = time_step.shape[1], tab.shape[3]
+    chains = turn.shape[1]
+    rows, width = residual.shape
+    pieces = len(gather_paths)
+    count, tp_count = sizes["z"] * sizes["y"], sizes["x"] * sizes["c"]
+    grid = tuple(sizes[name] for name in chip_axes)
+    blocks = math.prod(grid)
+    per = count // sizes["c"]
+    landing = []
+    for order in sum_paths:
+        for stage in range(3):
+            axis = order[stage]
+            left = tuple(sizes[name] for name in chip_axes if name not in order[: stage + 1])
+            landing.append(
+                pltpu.VMEM((max(sizes[axis] - 1, 1),) + left + (rows, width // pieces), jnp.bfloat16)
+            )
+    copies = 2 * pieces * sum(max(sizes[name] - 1, 0) for name in chip_axes)
+    small = max(count, tp_count)
+    vmem = pl.BlockSpec(memory_space=pltpu.VMEM)
+    far = pl.BlockSpec(memory_space=pl.ANY)
+    dma = pltpu.SemaphoreType.DMA
+    f32, bf16 = jnp.float32, jnp.bfloat16
+    return pl.pallas_call(
+        lambda *refs: layer_kernel(sizes, *refs),
+        name="whole_layer",
+        out_shape=jax.ShapeDtypeStruct((rows, width), bf16),
+        in_specs=[vmem] * 11 + [far] * 4,
+        out_specs=vmem,
+        scratch_shapes=[
+            pltpu.VMEM((channels, span), bf16),
+            pltpu.VMEM((2, span, 3 * groups), bf16),
+            pltpu.VMEM((chains, 2, span, lanes), f32),
+            pltpu.VMEM((chains, 2, span, lanes), f32),
+            pltpu.VMEM((3 * chains, lanes), f32),
+            pltpu.VMEM((count, 3 * chains, lanes), f32),
+            pltpu.VMEM((2, chains, lanes), f32),
+            pltpu.VMEM((span, channels), f32),
+            pltpu.VMEM((tp_count, rows, channels), f32),
+            pltpu.VMEM((tp_count,) + vec.shape, f32),
+            pltpu.VMEM(out_weight.shape, bf16),
+            pltpu.VMEM((rows, width), bf16),
+            pltpu.VMEM((taps.shape[0], unit), f32),
+            pltpu.VMEM((width, 2 * unit), bf16),
+            pltpu.VMEM((unit, width), bf16),
+            pltpu.VMEM(grid + (rows, width), bf16),
+            pltpu.VMEM((blocks + 2, rows + 16, 2 * unit), f32),
+            pltpu.VMEM((blocks * rows, unit), bf16),
+            pltpu.VMEM(grid + (rows, width), bf16),
+            *landing,
+            dma((1,)),
+            dma((4, small)),
+            dma((4, small)),
+            dma((3,)),
+            dma((copies,)),
+            dma((copies,)),
+            dma((3, per)),
+            dma((3, count)),
+            dma((3, per)),
+            dma((3, per)),
+        ],
+        compiler_params=pltpu.CompilerParams(
+            collective_id=2, has_side_effects=True, vmem_limit_bytes=63 * 1024 * 1024
+        ),
+    )(*arrays, *weights)
+
+
+def mesh_sizes(sp_count, tp_count):
+    cores = 2
+    across = tp_count // cores
+    deep = math.gcd(across, sp_count)
+    return {"z": sp_count // deep, "y": deep, "x": across, "c": cores}
+
+
+def tile_units(sizes, x_shape, in_shape, value_shape, down_shape, residual_shape):
+    count = sizes["z"] * sizes["y"]
+    unit = value_shape[1] * sizes["c"] // count
+    rows, width = residual_shape
+    span, states, head = x_shape[0], in_shape[3], in_shape[4]
+    fits = (
+        count % sizes["c"] == 0
+        and unit % 128 == 0
+        and 2 * unit % 256 == 0
+        and value_shape[0] % 16 == 0
+        and down_shape[1] % 128 == 0
+        and width % 512 == 0
+        and rows % 16 == 0
+        and span % 128 == 0
+        and 2 * states == 128
+        and in_shape[2] % 16 == 0
+        and width % (256 * len(gather_paths)) == 0
+        and head % 16 == 0
+        and x_shape[1] % 128 == 0
+    )
+    return unit if fits else 0
+
+
+def one_kernel(sizes, unit, args):
+    (
+        mixer_input,
+        time_step,
+        damping,
+        input_map,
+        readout,
+        skip_gain,
+        out_gain,
+        out_weight,
+        residual,
+        channel_gain,
+        value_weight,
+        gate_weight,
+        value_taps,
+        gate_taps,
+        down_weight,
+    ) = args
+    span = mixer_input.shape[0]
+    groups, states, head = input_map.shape[2:]
+    pairs = groups // 2
+    number = jnp.arange(states, dtype=jnp.float32)
+
+    def by_pair(array):
+        return array.reshape(2 * pairs, 2 * array.shape[-1])
+
+    near = jnp.arange(1, 9, dtype=jnp.float32)
+    reach = jnp.stack((near, near[::-1]))[:, :, None, None] * number
+    angle = math.pi * turns(time_step[:, None, :, None], reach)
+    tab = jnp.stack((jnp.cos(angle), jnp.sin(angle)))
+    tab = tab.reshape(2, 2, 8, pairs, 2 * states).transpose(1, 3, 0, 2, 4)
+    tab = tab.reshape(2 * pairs, 2, 8, 2 * states)
+    far = math.pi * turns(time_step[:, :, None], number * span)
+    scale = jnp.sqrt(-jnp.expm1(-time_step))
+    total = jnp.exp(-0.5 * span * time_step - jnp.sum(damping, axis=1))
+    turn = jnp.stack(
+        [
+            by_pair(jnp.broadcast_to(item, far.shape))
+            for item in (jnp.cos(far), jnp.sin(far), scale[:, :, None], total[:, :, None])
+        ]
+    )
+    same = jnp.eye(2, dtype=jnp.float32)
+    in_map = input_map.reshape(2, 2, pairs, 2, states, head).transpose(2, 3, 5, 0, 1, 4)
+    in_map = in_map[:, :, :, :, :, None, :] * same[:, None, None, None, :, None].astype(
+        in_map.dtype
+    )
+    in_map = in_map.reshape(pairs, 2 * head, 8 * states)
+    signed = jnp.stack((readout[:, 0], -readout[:, 1]), axis=1)
+    out_map = signed.reshape(2, 2, pairs, 2, head, states).transpose(2, 3, 4, 0, 1, 5)
+    out_map = out_map[:, :, :, :, :, None, :] * same[:, None, None, None, :, None]
+    out_map = out_map.reshape(pairs, 2 * head, 8 * states)
+    vec = jnp.pad(jnp.stack((out_gain, skip_gain)), ((0, 6), (0, 0)))
+    taps = jnp.pad(jnp.concatenate((value_taps, gate_taps)), ((0, 2), (0, 0)))
+    arrays = (
+        mixer_input,
+        time_step,
+        damping,
+        tab,
+        turn,
+        in_map,
+        out_map,
+        vec,
+        taps,
+        residual,
+        channel_gain.reshape(1, -1),
+    )
+    return whole_layer(
+        sizes, arrays, (out_weight, value_weight, gate_weight, down_weight), unit
+    )
+
+
 def body(
     mixer_input,
     time_step,
@@ -401,6 +1103,19 @@
     down_weight,
 ):
     count, mine = lax.axis_size("sp"), lax.axis_index("sp")
+    sizes = mesh_sizes(count, lax.axis_size("tp"))
+    unit = tile_units(
+        sizes,
+        mixer_input.shape,
+        input_map.shape,
+        value_weight.shape,
+        down_weight.shape,
+        residual.shape,
+    )
+    if unit:
+        args = (mixer_input, time_step, damping, input_map, readout, skip_gain, out_gain)
+        args += (out_weight, residual, channel_gain, value_weight, gate_weight)
+        return one_kernel(sizes, unit, args + (value_taps, gate_taps, down_weight))
     depth, hidden_width = value_weight.shape
     part = hidden_width // count
     up_send = jnp.concatenate(

time: 169 us -> 126 us (0.75)
  Pallas kernels: 128 us -> 112 us
  other arithmetic: 15.9 us -> 6.55 us
  matrix products: 9.03 us -> 0 us
  local copies, waits for them, and re-layouts: 10.9 us -> 7.18 us
  starting transfers between devices: 3.34 us -> 0 us
    pallas_call x2 -> x1, Pallas kernels: 128 us -> 112 us  [whole_layer(): pl.pallas_call(lambda *refs: layer_kernel(sizes, *refs), name='whole_laye...]
    dot_general x6 -> x0, matrix products: 9.03 us -> none  [the longest x1 3.18 us: body(): jnp.dot(normed_mix, out_weight, preferred_element_type=jnp.float32)]
    add x4 -> x1, other arithmetic: 5.29 us -> 0.01 us  [one_kernel(): near = jnp.arange(1, 9, dtype=jnp.float32)]
    sub x2 -> x0, other arithmetic: 4.5 us -> none  [the longest x1 4.5 us: mixer(): state = jnp.concatenate((cos * re - sin * im, cos * im + sin * re), axis=3)]
    all_to_all x1 -> x0, starting transfers between devices: 3.34 us -> none  [body(): lax.all_to_all(mixed_y, 'tp', split_axis=0, concat_axis=0, tiled=True)]
    unnamed x24 -> x14, local copies, waits for them, and re-layouts: 5.59 us -> 2.36 us
    concatenate x5 -> x1, other arithmetic: 3.76 us -> 0.63 us  [one_kernel(): taps = jnp.pad(jnp.concatenate((value_taps, gate_taps)), ((0, 2), (0, 0)))]
    mul x0 -> x16, local copies, waits for them, and re-layouts: none -> 3.06 us  [the longest x4 1.58 us: one_kernel(): out_map[:, :, :, :, :, None, :] * same[:, None, None, None, :, None]]
  transfers between devices with their start and end apart: 1 -> 0, of which waited for: 0 -> 0; matrix products, arithmetic and copies ran while one was open for 3% -> 0% of each run, Pallas kernels for 0% -> 0%
where the time goes in v1:
time: 126 us
  Pallas kernels  112 us (89%)
  local copies, waits for them, and re-layouts  7.18 us (6%)
  other arithmetic  6.55 us (5%)
    pallas_call x1, Pallas kernels, whole_layer(): pl.pallas_call(lambda *refs: layer_kernel(sizes, *refs), name='whole_laye...  112 us

profile of v1, /device:TPU:0, one launch (start us, length us, event | category | flops | bytes accessed | tf_op | source)
XLA Modules:
  0.0 125.9 jit_solution(13292887818862138903)
XLA Ops:
  0.0 0.8 reduce_sum.9
  0.8 0.7 negate_sqrt_fusion
  2.1 0.6 pad_maximum_fusion.refs_4_
  3.0 0.1 reverse.3
  3.3 0.3 fusion.1
  3.6 0.7 copy.19
  4.3 1.1 fusion.6
  5.5 0.4 copy.21
  5.9 0.4 mul.341
  6.2 0.9 mul.342
  7.2 0.1 mul.343
  7.3 0.2 mul.344
  7.5 0.9 broadcast_multiply_fusion.refs_6_
  8.3 0.3 copy.20
  8.6 0.4 mul.335
  9.0 0.3 mul.336
  9.4 0.1 mul.337
  9.5 0.1 mul.338
  9.6 0.7 broadcast_multiply_fusion.1.refs_5_
  10.3 0.8 copy.22.refs_2_
  11.1 0.6 select_maximum_fusion.refs_8_
  11.7 0.6 select_maximum_fusion.1.refs_7_
  12.3 112.0 %whole_layer.1 = bf16[32,2048]{1,0:T(8,128)(2,1)} custom-call(bf16[128,256]{1,0:T(8,128)(2,1)} %refs_0_.1, f32[2,16]{1,0:T(2,128)} %refs_1_.1, f32[2,128,16]{2,1,0:T(8,128)} %copy.22.refs_2_, f32[16,2,8,128]{3,2,1,0:T(8,128)} %bitcast.19, f32[4,16,128]{2,1,0:T(8,128)} %pad_maximum_fusion.refs_4_, bf16[8,32,512]{2,1,0:T(8,128)(2,1)} %broadcast_multiply_fusion.1.refs_5_, ...), custom_call_target="tpu_custom_call" | custom-call | tf_op jit(solution)/shard_map/whole_layer/pallas_call | solution.py:943
  124.4 1.6 %copy.24 = bf16[32,2048]{1,0:T(8,128)(2,1)} copy(bf16[32,2048]{1,0:T(8,128)(2,1)} %whole_layer.1) | data formatting | bytes 262144
  (36 shorter events, 1.2 us)
Async XLA Ops:
  3.3 5.0 %copy-start = (bf16[2,2,16,64,16]{3,4,2,1,0:T(8,128)(2,1)S(1)}, bf16[2,2,16,64,16]{3,4,2,1,0:T(8,128)(2,1)}, u32[]{:S(2)}) copy-start(bf16[2,2,16,64,16]{3,4,2,1,0:T(8,128)(2,1)} %param.18) | copy-start | bytes 393220
  5.4 4.9 %copy-start.1 = (f32[2,128,16]{1,2,0:T(8,128)S(1)}, f32[2,128,16]{1,2,0:T(8,128)}, u32[]{:S(2)}) copy-start(f32[2,128,16]{1,2,0:T(8,128)} %param.17) | copy-start | bytes 49156
  5.4 5.7 %copy-start.2 = (f32[3,1536]{1,0:T(4,128)S(1)}, f32[3,1536]{1,0:T(4,128)}, u32[]{:S(2)}) copy-start(f32[3,1536]{1,0:T(4,128)} %param.28) | copy-start | bytes 55300
  5.4 5.7 %copy-start.3 = (f32[3,1536]{1,0:T(4,128)S(1)}, f32[3,1536]{1,0:T(4,128)}, u32[]{:S(2)}) copy-start(f32[3,1536]{1,0:T(4,128)} %param.27) | copy-start | bytes 55300
  5.4 6.3 %copy-start.4 = (f32[256]{0:T(256)S(1)}, f32[256]{0:T(256)}, u32[]{:S(2)}) copy-start(f32[256]{0:T(256)} %param.20) | copy-start | bytes 3076
  5.4 6.3 %copy-start.5 = (f32[256]{0:T(256)S(1)}, f32[256]{0:T(256)}, u32[]{:S(2)}) copy-start(f32[256]{0:T(256)} %param.21) | copy-start | bytes 3076

commit v2 on v1

--- a/solution.py
+++ b/solution.py
@@ -384,8 +384,48 @@
 
 
 gather_paths = (("z", "y", "x"), ("z", "x", "y")) * 2
-sum_paths = (("x", "y", "z"), ("y", "x", "z")) * 2
+sum_paths = (("x", "y", "z"), ("y", "x", "z")) * 4
+halves = 2
 chip_axes = ("z", "y", "x")
+
+
+def turned(turn):
+    turn = turn - 2.0 * jnp.floor(turn * 0.5)
+    quarter = jnp.floor(2.0 * turn + 0.5)
+    angle = math.pi * (turn - 0.5 * quarter)
+    square = angle * angle
+    sin = angle + angle * square * (
+        -1.6666654611e-1 + square * (8.3321608736e-3 - 1.9515295891e-4 * square)
+    )
+    cos = (
+        1.0
+        - 0.5 * square
+        + square
+        * square
+        * (4.166664568298827e-2 + square * (-1.388731625493765e-3 + 2.443315711809948e-5 * square))
+    )
+    swap = (quarter == 1.0) | (quarter == 3.0)
+    full_cos = jnp.where(swap, sin, cos)
+    full_sin = jnp.where(swap, cos, sin)
+    full_cos = jnp.where((quarter == 1.0) | (quarter == 2.0), -full_cos, full_cos)
+    full_sin = jnp.where((quarter == 2.0) | (quarter == 3.0), -full_sin, full_sin)
+    return full_cos, full_sin
+
+
+def turns_of(step_size, count):
+    coarse = jnp.floor(step_size * 1024.0 + 0.5) * (1.0 / 1024.0)
+    whole = coarse * count
+    whole = whole - 2.0 * jnp.floor(whole * 0.5)
+    return whole + (step_size - coarse) * count
+
+
+def drive_scale(step_size):
+    series = 1.0 / 720.0
+    for term in (120.0, 24.0, 6.0, 2.0, 1.0):
+        series = 1.0 / term - step_size * series
+    return jnp.sqrt(
+        jnp.where(step_size < 0.25, step_size * series, 1.0 - jnp.exp(-step_size))
+    )
 
 
 def layer_kernel(sizes, *refs):
@@ -393,12 +433,12 @@
         x_ref,
         step_ref,
         damping_ref,
-        tab_ref,
-        turn_ref,
         in_ref,
         readout_ref,
-        vec_ref,
-        taps_ref,
+        skip_ref,
+        gain_ref,
+        value_taps_ref,
+        gate_taps_ref,
         residual_ref,
         channel_ref,
         out_w_hbm,
@@ -410,24 +450,31 @@
         decay_parts,
         local,
         carried,
+        tab_ref,
+        turn_ref,
+        totals,
+        totals_all,
+        ends,
         packet,
         packets,
         carry,
         y_all,
         y_land,
-        vec_all,
+        gain_all,
         out_w,
         state_rows,
         taps,
         up_w,
         down_w,
+        held_up,
+        held_down,
         rows_all,
         up_rows,
         hidden_rows,
         partial,
-    ) = refs[:35]
-    pieces = len(gather_paths)
-    landing = refs[35 : 35 + 3 * pieces]
+    ) = refs[:42]
+    sums_in = len(sum_paths)
+    landing = refs[42 : 42 + 3 * sums_in]
     (
         local_sem,
         small_send,
@@ -435,20 +482,26 @@
         taps_sem,
         hop_send,
         hop_recv,
+        line_send,
+        line_recv,
+        hold_send,
+        hold_recv,
         w_send,
         w_recv,
         f_send,
         f_recv,
-    ) = refs[35 + 3 * pieces :]
+    ) = refs[42 + 3 * sums_in :]
     span, channels = x_ref.shape
-    pairs, heads, lanes = in_ref.shape[0], in_ref.shape[1], tab_ref.shape[3]
-    groups = step_ref.shape[1]
+    groups, head, states = in_ref.shape[2:]
+    pairs, heads, lanes = groups // 2, 2 * head, 2 * states
     tiles = span // 8
+    pieces = len(gather_paths)
     rows, width = residual_ref.shape
     piece_width = width // pieces
     depth = value_hbm.shape[0]
     part = down_hbm.shape[1]
-    unit = taps.shape[1]
+    sub = part // halves
+    unit = taps.shape[2]
     cores = sizes["c"]
     count, tp_count = sizes["z"] * sizes["y"], sizes["x"] * cores
     per = count // cores
@@ -498,102 +551,203 @@
     pl.semaphore_wait(barrier, greeted)
 
     def block_view(kind, source):
-        if kind == 2:
-            return down_w.at[:, pl.ds(pl.multiple_of(source * part, part), part)]
+        if kind >= 2:
+            return down_w.at[kind - 2, :, pl.ds(pl.multiple_of(source * sub, sub), sub)]
         column = kind * unit
         return up_w.at[pl.ds(pl.multiple_of(source * depth, depth), depth), pl.ds(column, unit)]
 
-    keeper = lax.rem(sp, cores)
-
-    def weight_copy(kind, slot):
-        place = lax.rem(slot + sp, per)
-        chip = core * per + place
+    layers = per // sizes["y"]
+    across = range(per - layers)
+    straight = range(per - layers, per)
+
+    def cut_of(kind, slot, side):
+        place = lax.rem(mine["z"] + slot, layers) * sizes["y"] + side
         start = pl.multiple_of(place * unit, unit)
-        if kind == 2:
-            source = down_hbm.at[pl.ds(start, unit), :]
+        if kind >= 2:
+            source = down_hbm.at[pl.ds(start, unit), pl.ds((kind - 2) * sub, sub)]
         else:
             source = (value_hbm, gate_hbm)[kind].at[:, pl.ds(start, unit)]
+        return core * per + place, source
+
+    def weight_copy(kind, slot):
+        shift = (slot // layers + 1) % sizes["y"]
+        chip, source = cut_of(kind, slot, mine["y"])
+        from_y = lax.rem(mine["y"] + sizes["y"] - shift, sizes["y"])
+        origin = mine["z"] * sizes["y"] + from_y
+        keeper = lax.rem(origin, cores)
+        if shift:
+            source = (held_down.at[slot, kind - 2] if kind >= 2 else held_up.at[slot, kind])
         stays = (chip == sp) & (keeper == core)
-        target = block_view(kind, sp)
+        target = block_view(kind, origin)
         device = (chip, mine["x"] * cores + keeper)
 
         def here():
-            return pltpu.make_async_copy(source, target, w_recv.at[kind, sp])
+            return pltpu.make_async_copy(source, target, w_recv.at[kind, origin // cores])
 
         def away():
-            return remote(source, target, w_send.at[kind, slot], w_recv.at[kind, sp], device)
+            return remote(source, target, w_send.at[kind, slot], w_recv.at[kind, origin // cores], device)
 
         return stays, here, away
+
+    def hold_copy(kind, slot):
+        side = lax.rem(mine["y"] + slot // layers + 1, sizes["y"])
+        _, source = cut_of(kind, slot, side)
+        held = held_down.at[slot, kind - 2] if kind >= 2 else held_up.at[slot, kind]
+        device = (mine["z"] * sizes["y"] + side, tp)
+        return remote(source, held, hold_send.at[kind, slot], hold_recv.at[kind, slot], device)
+
+    def hand_over(kinds, slots):
+        for slot in slots:
+            for kind in kinds:
+                hold_copy(kind, slot).start()
 
     def send_weights(kinds, slots):
         for slot in slots:
             for kind in kinds:
+                if slot in across:
+                    hold_copy(kind, slot).wait_recv()
                 stays, here, away = weight_copy(kind, slot)
                 pl.when(stays)(lambda: here().start())
                 pl.when(jnp.logical_not(stays))(lambda: away().start())
 
     def finish_sends():
         for slot in range(per):
-            for kind in range(3):
+            for kind in range(2 + halves):
+                if slot in across:
+                    hold_copy(kind, slot).wait_send()
                 stays, _, away = weight_copy(kind, slot)
                 pl.when(jnp.logical_not(stays))(lambda: away().wait_send())
+
+    def passed_on(kinds, side, index):
+        source = side + cores * index
+        if kinds[0] >= 2:
+            view = block_view(kinds[0], source)
+        else:
+            view = up_w.at[pl.ds(pl.multiple_of(source * depth, depth), depth), :]
+        at = max(kinds[0] - 1, 0)
+        return remote(view, view, f_send.at[at, index], f_recv.at[at, index], partner)
 
     def forward_weights(kinds):
         started = []
         for index in range(per):
             for kind in kinds:
-                source = core + cores * index
-                view = block_view(kind, source)
-                remote(view, view, w_send.at[kind, 0], w_recv.at[kind, source], partner).wait_recv()
-                copy = remote(view, view, f_send.at[kind, index], f_recv.at[kind, index], partner)
-                copy.start()
-                started.append(copy)
+                view = block_view(kind, core + cores * index)
+                remote(view, view, w_send.at[kind, 0], w_recv.at[kind, index], partner).wait_recv()
+            copy = passed_on(kinds, core, index)
+            copy.start()
+            started.append(copy)
         return started
 
     def forwarded(kinds, started):
         for copy in started:
             copy.wait_send()
         for index in range(per):
-            for kind in kinds:
-                view = block_view(kind, lax.rem(core + 1, cores) + cores * index)
-                remote(view, view, f_send.at[kind, index], f_recv.at[kind, index], partner).wait_recv()
-
-    send_weights((0,), (0,))
-
-    vec_copies = []
+            passed_on(kinds, lax.rem(core + 1, cores), index).wait_recv()
+
+    hand_over((0,), across[:1])
+    send_weights((0,), straight[:1])
+
+    early_copies = []
+
+    sends_at = {"gain": 0, "total": tp_count, "carry": tp_count + count}
+    sends_at["y"] = sends_at["edge"] = sends_at["carry"]
+    lands_at = dict(sends_at)
+    lands_at["y"] = lands_at["carry"] + count
+    lands_at["edge"] = lands_at["y"] + tp_count
+
+    def small(source, target, kind, index, device):
+        send = small_send.at[sends_at[kind] + index - 1]
+        return remote(source, target, send, small_recv.at[lands_at[kind] + index - 1], device)
+
     for offset in range(1, tp_count):
-        copy = remote(
-            vec_ref,
-            vec_all.at[tp],
-            small_send.at[0, offset],
-            small_recv.at[0, offset],
-            (sp, lax.rem(tp + offset, tp_count)),
+        peer = (sp, lax.rem(tp + offset, tp_count))
+        copy = small(gain_ref, gain_all.at[tp], "gain", offset, peer)
+        copy.start()
+        early_copies.append(copy)
+    gain_all[tp] = gain_ref[...]
+
+    owns_taps = core == sp // per
+    taps_start = pl.ds(pl.multiple_of(lax.rem(sp, per) * unit, unit), unit)
+    taps_copies = []
+    for kind, source in enumerate((value_taps_ref, gate_taps_ref)):
+        view = source.at[:, taps_start]
+        keep = pltpu.make_async_copy(view, taps.at[kind], taps_sem.at[3 * kind])
+        send = remote(
+            view, taps.at[kind], taps_sem.at[3 * kind + 1], taps_sem.at[3 * kind + 2], partner
         )
-        copy.start()
-        vec_copies.append(copy)
-    vec_all[tp] = vec_ref[...]
-
-    owns_taps = core == sp // per
-    taps_view = taps_ref.at[:, pl.ds(pl.multiple_of(lax.rem(sp, per) * unit, unit), unit)]
-    taps_keep = pltpu.make_async_copy(taps_view, taps, taps_sem.at[0])
-    taps_send = remote(taps_view, taps, taps_sem.at[1], taps_sem.at[2], partner)
+        taps_copies.append((keep, send))
 
     @pl.when(owns_taps)
     def _():
-        taps_keep.start()
-        taps_send.start()
-
-    x_t[...] = jnp.transpose(x_ref[...].astype(jnp.float32)).astype(jnp.bfloat16)
+        for keep, send in taps_copies:
+            keep.start()
+            send.start()
+
+    pick_group = lax.broadcasted_iota(jnp.int32, (groups, lanes), 0)
+    pick_side = lax.broadcasted_iota(jnp.int32, (groups, lanes), 1) // states
+    pick_odd = (lax.rem(pick_group, 2) == pick_side).astype(jnp.bfloat16)
+    own_pair = lax.broadcasted_iota(
+        jnp.int32, (pairs, groups), 1
+    ) // 2 == lax.broadcasted_iota(jnp.int32, (pairs, groups), 0)
+
+    def over_lanes(row):
+        left = jnp.where(own_pair, jnp.broadcast_to(row, (pairs, groups)), 0.0)
+        found = jnp.zeros((pairs, lanes), jnp.float32)
+        for _ in range(3):
+            rounded = left.astype(jnp.bfloat16)
+            found = found + jnp.dot(rounded, pick_odd, preferred_element_type=jnp.float32)
+            left = left - rounded.astype(jnp.float32)
+        return found
+
+    number = lax.rem(lax.broadcasted_iota(jnp.int32, (8, lanes), 1), states).astype(jnp.float32)
+    near = lax.broadcasted_iota(jnp.int32, (8, lanes), 0).astype(jnp.float32)
     for k in range(2):
-        left = jnp.exp(-0.5 * step_ref[k : k + 1, :] - damping_ref[k])
+        step_size = step_ref[k : k + 1, :]
+        log_decay = -0.5 * step_size - jnp.transpose(damping_ref[k])
+        rows_at = pl.ds(k * pairs, pairs)
+        totals[rows_at, :] = over_lanes(jnp.exp(jnp.sum(log_decay, axis=0, keepdims=True)))
+        left = jnp.exp(log_decay)
         for level in range(3):
             rounded = left.astype(jnp.bfloat16)
             decay_parts[k, :, level * groups : (level + 1) * groups] = rounded
             left = left - rounded.astype(jnp.float32)
-
+    total_copies = []
+    for offset in range(1, count):
+        peer = (lax.rem(sp + offset, count), tp)
+        copy = small(totals, totals_all.at[sp], "total", offset, peer)
+        copy.start()
+        total_copies.append(copy)
+    totals_all[sp] = totals[...]
+    for k in range(2):
+        step_size = step_ref[k : k + 1, :]
+        rows_at = pl.ds(k * pairs, pairs)
+        wide_step = over_lanes(step_size)
+        turn_ref[2, rows_at, :] = over_lanes(drive_scale(step_size))
+        cos, sin = turned(turns_of(wide_step, number * span))
+        turn_ref[0, rows_at, :] = cos
+        turn_ref[1, rows_at, :] = sin
+        reach = near + 1.0 if k == 0 else 8.0 - near
+        for pair in range(pairs):
+            cos, sin = turned(turns_of(wide_step[pair : pair + 1], number * reach))
+            tab_ref[k * pairs + pair, 0] = cos
+            tab_ref[k * pairs + pair, 1] = sin
+
+    x_t[...] = jnp.transpose(x_ref[...].astype(jnp.float32)).astype(jnp.bfloat16)
     row_in_tile = lax.broadcasted_iota(jnp.int32, (1, 8, lanes), 1)
     pick_row = lax.rem(lax.broadcasted_iota(jnp.int32, (3 * groups, lanes), 0), groups)
     pick_lane = lax.broadcasted_iota(jnp.int32, (3 * groups, lanes), 1) // (lanes // 2)
+
+    def both_groups(ref, pair):
+        blocks_of = []
+        empty = jnp.zeros((head, states), jnp.float32)
+        for k in range(2):
+            for kind in range(2):
+                first = ref[k, kind, 2 * pair].astype(jnp.float32)
+                second = ref[k, kind, 2 * pair + 1].astype(jnp.float32)
+                upper = jnp.concatenate((first, empty), axis=1)
+                lower = jnp.concatenate((empty, second), axis=1)
+                blocks_of.append(jnp.concatenate((upper, lower), axis=0))
+        return jnp.concatenate(blocks_of, axis=1)
 
     def chain(k, at, start_real, start_imag):
         real, imag = start_real, start_imag
@@ -612,7 +766,10 @@
     def first_pass(pair, _):
         inputs = x_t[pl.ds(pl.multiple_of(pair * heads, heads), heads), :]
         driven = lax.dot_general(
-            inputs, in_ref[pair], (((0,), (0,)), ((), ())), preferred_element_type=jnp.float32
+            inputs,
+            both_groups(in_ref, pair).astype(jnp.bfloat16),
+            (((0,), (0,)), ((), ())),
+            preferred_element_type=jnp.float32,
         )
         for k in range(2):
             at = k * pairs + pair
@@ -643,29 +800,26 @@
             at = k * pairs + pair
             none = jnp.zeros((8, lanes), jnp.float32)
             real, imag = chain(k, at, none, none)[1:]
-            packet[pl.ds(at, 1), :] = real[0:1]
-            packet[pl.ds(2 * pairs + at, 1), :] = imag[0:1]
+            ends[pl.ds(at, 1), :] = real[0:1]
+            ends[pl.ds(2 * pairs + at, 1), :] = imag[0:1]
         return _
 
-    packet[pl.ds(4 * pairs, 2 * pairs), :] = turn_ref[3]
     lax.fori_loop(0, pairs, first_pass, 0)
 
+    packet[...] = ends[...].astype(jnp.bfloat16)
     packets[sp] = packet[...]
     carry_copies = []
     for offset in range(1, count):
-        copy = remote(
-            packet,
-            packets.at[sp],
-            small_send.at[1, offset],
-            small_recv.at[1, offset],
-            (lax.rem(sp + offset, count), tp),
-        )
+        peer = (lax.rem(sp + offset, count), tp)
+        copy = small(packet, packets.at[sp], "carry", offset, peer)
         copy.start()
         carry_copies.append(copy)
-    send_weights((1,), (0,))
-    send_weights((0, 1), (1,))
-    for copy in carry_copies:
+    for copy in total_copies + carry_copies:
         copy.wait()
+    hand_over((1,), across[:1])
+    hand_over((0, 1), across[1:])
+    send_weights((1,), straight[:1])
+    send_weights((0,), straight[1:])
 
     for k in range(2):
         at = pl.ds(k * pairs, pairs)
@@ -673,20 +827,19 @@
         real = jnp.zeros((pairs, lanes), jnp.float32)
         imag = real
         for index in range(count) if k == 0 else range(count - 1, -1, -1):
-            total = packets[index, pl.ds((4 + k) * pairs, pairs), :]
+            total = totals_all[index, at, :]
+            end = packets[index].astype(jnp.float32)
+            end_real = end[k * pairs : (k + 1) * pairs]
+            end_imag = end[(2 + k) * pairs : (3 + k) * pairs]
             turned_real = cos * real - sin * imag
             turned_imag = cos * imag + sin * real
             before = (index < sp) if k == 0 else (index > sp)
-            real = jnp.where(before, packets[index, at, :] + total * turned_real, real)
-            imag = jnp.where(
-                before,
-                packets[index, pl.ds((2 + k) * pairs, pairs), :] + total * turned_imag,
-                imag,
-            )
+            real = jnp.where(before, end_real + total * turned_real, real)
+            imag = jnp.where(before, end_imag + total * turned_imag, imag)
         carry[0, at, :] = real
         carry[1, at, :] = imag
 
-    gains = vec_ref[1:2, :] * x_ref[...].astype(jnp.float32)
+    gains = skip_ref[...] * x_ref[...].astype(jnp.float32)
     for pair in range(pairs):
         parts = []
         for k in range(2):
@@ -699,7 +852,8 @@
         state = jnp.concatenate(parts, axis=1)
         state_high = state.astype(jnp.bfloat16)
         state_low = (state - state_high.astype(jnp.float32)).astype(jnp.bfloat16)
-        out_map = readout_ref[pair]
+        sign = jnp.concatenate([jnp.full((1, lanes), v, jnp.float32) for v in (1, -1, 1, -1)], axis=1)
+        out_map = both_groups(readout_ref, pair) * sign
         map_high = out_map.astype(jnp.bfloat16)
         map_low = (out_map - map_high.astype(jnp.float32)).astype(jnp.bfloat16)
 
@@ -715,22 +869,17 @@
     y_copies = []
     for offset in range(1, tp_count):
         peer = lax.rem(tp + offset, tp_count)
-        copy = remote(
-            y_all.at[pl.ds(pl.multiple_of(peer * rows, rows), rows), :],
-            y_land.at[tp],
-            small_send.at[2, offset],
-            small_recv.at[2, offset],
-            (sp, peer),
-        )
+        part_rows = y_all.at[pl.ds(pl.multiple_of(peer * rows, rows), rows), :]
+        copy = small(part_rows, y_land.at[tp], "y", offset, (sp, peer))
         copy.start()
         y_copies.append(copy)
     y_land[tp] = y_all[pl.ds(pl.multiple_of(tp * rows, rows), rows), :]
-    for copy in vec_copies + y_copies:
+    for copy in early_copies + y_copies:
         copy.wait()
     out_copy.wait()
 
     mixed = jnp.concatenate([y_land[peer] for peer in range(tp_count)], axis=1)
-    gain = jnp.concatenate([vec_all[peer, 0:1, :] for peer in range(tp_count)], axis=1)
+    gain = jnp.concatenate([gain_all[peer] for peer in range(tp_count)], axis=1)
     inverse = lax.rsqrt(jnp.mean(mixed * mixed, axis=1, keepdims=True) + norm_eps)
     normed_mix = (mixed * inverse * gain).astype(jnp.bfloat16)
     square = jnp.zeros((rows, 1), jnp.float32)
@@ -746,10 +895,60 @@
     normed = state_rows[...].astype(jnp.float32) * scale_rows * channel_ref[...]
     rows_all[mine["z"], mine["y"], mine["x"]] = normed.astype(jnp.bfloat16)
 
+    deep = sizes["z"] // 2
+    base = mine["z"] // deep * deep
+    other = deep - base
+    relays = mine["z"] == deep - 1 + base // deep
+    far_end = deep - base // deep
+
+    def plane(z):
+        return z * sizes["y"] + mine["y"], tp
+
+    def line_copy(piece, source, target, at):
+        columns = pl.ds(piece * piece_width, piece_width)
+        view = rows_all.at[source, mine["y"], mine["x"], :, columns]
+        return remote(
+            view, view, line_send.at[piece, at], line_recv.at[piece, source], plane(target)
+        )
+
+    def line_start(piece):
+        line_copy(piece, mine["z"], far_end, 0).start()
+        for offset in range(1, deep):
+            line_copy(piece, mine["z"], base + lax.rem(mine["z"] + offset, deep), offset).start()
+
+    def line_relay(piece, action):
+        for index in range(deep):
+            for offset in range(1, deep):
+                at = deep + index * (deep - 1) + offset - 1
+                target = base + lax.rem(mine["z"] + offset, deep)
+                copy = line_copy(piece, other + index, target, at)
+                copy.start() if action == "start" else copy.wait_send()
+
+    def line_finish(piece):
+        for index in range(deep):
+            line_copy(piece, other + index, far_end, 0).wait_recv()
+        pl.when(relays)(lambda: line_relay(piece, "start"))
+        for offset in range(1, deep):
+            source = base + lax.rem(mine["z"] + offset, deep)
+            line_copy(piece, source, far_end, 0).wait_recv()
+
+    def line_sent(piece):
+        for at in range(deep):
+            line_copy(piece, mine["z"], far_end, at).wait_send()
+        pl.when(relays)(lambda: line_relay(piece, "sent"))
+
+    for piece in range(pieces):
+        line_start(piece)
+
+    send_weights((1,), straight[1:])
+
     slot = 0
+    sums_at = pieces * (sizes["y"] + sizes["x"] - 2)
     pending = [[] for _ in range(pieces)]
-    for stage in range(3):
+    for stage in range(1, 3):
         for piece in range(pieces):
+            if stage == 1:
+                line_finish(piece)
             axis = gather_paths[piece][stage]
             done = gather_paths[piece][:stage]
             for copy in pending[piece]:
@@ -763,13 +962,17 @@
                 copy.start()
                 pending[piece].append(copy)
                 slot += 1
-        if stage == 0:
-            send_weights((0, 1), range(2, per))
-            send_weights((2,), range(per))
+        if stage == 1:
+            send_weights((0, 1), across)
+    for kind in range(2, 2 + halves):
+        hand_over((kind,), across)
+        send_weights((kind,), straight)
     up_started = forward_weights((0, 1))
     for piece in range(pieces):
         for copy in pending[piece]:
             copy.wait()
+    for piece in range(pieces):
+        line_sent(piece)
     forwarded((0, 1), up_started)
 
     @pl.when(core == 0)
@@ -792,27 +995,25 @@
 
     lax.fori_loop(0, 2 * unit // chunk, project, 0)
 
+    send_weights((2,), across)
     edges = []
     for kind, (take, land, first) in enumerate(((rows, 0, 1 + core), (8, rows + 8, core))):
-        copy = remote(
-            up_rows.at[pl.ds(1, blocks), pl.ds(take, 8), :],
-            up_rows.at[pl.ds(first, blocks), pl.ds(land, 8), :],
-            small_send.at[3, kind],
-            small_recv.at[3, kind],
-            partner,
-        )
+        edge = up_rows.at[pl.ds(1, blocks), pl.ds(take, 8), :]
+        beyond = up_rows.at[pl.ds(first, blocks), pl.ds(land, 8), :]
+        copy = small(edge, beyond, "edge", kind + 1, partner)
         copy.start()
         edges.append(copy)
-    down_started = forward_weights((2,))
 
     @pl.when(owns_taps)
     def _():
-        taps_keep.wait()
-        taps_send.wait_send()
+        for keep, send in taps_copies:
+            keep.wait()
+            send.wait_send()
 
     @pl.when(jnp.logical_not(owns_taps))
     def _():
-        taps_send.wait_recv()
+        for _, send in taps_copies:
+            send.wait_recv()
 
     for copy in edges:
         copy.wait()
@@ -820,21 +1021,25 @@
     def mix(b, _):
         window = up_rows[b + 1]
 
-        def conv(base, columns):
+        def conv(kind, columns):
             return (
-                taps[base : base + 1, :] * window[7 : rows + 7, columns]
-                + taps[base + 1 : base + 2, :] * window[8 : rows + 8, columns]
-                + taps[base + 2 : base + 3, :] * window[9 : rows + 9, columns]
+                taps[kind, 0:1, :] * window[7 : rows + 7, columns]
+                + taps[kind, 1:2, :] * window[8 : rows + 8, columns]
+                + taps[kind, 2:3, :] * window[9 : rows + 9, columns]
             )
 
         value = conv(0, slice(0, unit))
-        gate = conv(3, slice(unit, 2 * unit))
+        gate = conv(1, slice(unit, 2 * unit))
         hidden = value * (gate / (1.0 + jnp.exp(-gate)))
         hidden_rows[pl.ds(pl.multiple_of(b * rows, rows), rows), :] = hidden.astype(jnp.bfloat16)
         return _
 
     lax.fori_loop(0, blocks, mix, 0)
-    forwarded((2,), down_started)
+
+    for kind in range(3, 2 + halves):
+        send_weights((kind,), across)
+    sum_width = width // sums_in
+    per_half = sums_in // halves
 
     def start_sum(piece, stage, slot):
         axis = sum_paths[piece][stage]
@@ -847,7 +1052,7 @@
                 for name in chip_axes
             )
             copy = remote(
-                partial.at[index + (slice(None), pl.ds(piece * piece_width, piece_width))],
+                partial.at[index + (slice(None), pl.ds(piece * sum_width, sum_width))],
                 landing[piece * 3 + stage].at[offset - 1],
                 hop_send.at[slot],
                 hop_recv.at[slot],
@@ -862,7 +1067,7 @@
         axis = sum_paths[piece][stage]
         done = sum_paths[piece][: stage + 1]
         land = landing[piece * 3 + stage]
-        columns = pl.ds(piece * piece_width, piece_width)
+        columns = pl.ds(piece * sum_width, sum_width)
         free = [name for name in chip_axes if name not in done]
 
         def add(step, _):
@@ -882,9 +1087,13 @@
             if free:
                 partial[index] = value.astype(jnp.bfloat16)
             else:
-                out_ref[:, columns] = (
-                    state_rows[:, columns].astype(jnp.float32) + value
-                ).astype(jnp.bfloat16)
+                for step_at in range(sum_width // sub):
+                    place = piece % per_half * sum_width // sub + step_at
+                    real = pl.ds(place * part + piece // per_half * sub, sub)
+                    added = value[:, step_at * sub : (step_at + 1) * sub]
+                    out_ref[:, real] = (
+                        state_rows[:, real].astype(jnp.float32) + added
+                    ).astype(jnp.bfloat16)
             return _
 
         if free:
@@ -892,36 +1101,54 @@
         else:
             add(0, 0)
 
-    slot = hop_send.shape[0] // 2
-    pending = []
-    for piece in range(pieces):
-        columns = pl.ds(piece * piece_width, piece_width)
-        sums = jnp.dot(hidden_rows[...], down_w[:, columns], preferred_element_type=jnp.float32)
-        shape = partial.shape[:3] + (rows, piece_width)
-        partial[:, :, :, :, columns] = sums.astype(jnp.bfloat16).reshape(shape)
-        started, slot = start_sum(piece, 0, slot)
-        pending.append(started)
-    for stage in range(1, 3):
-        for piece in range(pieces):
-            for copy in pending[piece]:
-                copy.wait()
-            add_landed(piece, stage - 1)
-            pending[piece], slot = start_sum(piece, stage, slot)
-    for piece in range(pieces):
-        for copy in pending[piece]:
-            copy.wait()
-        add_landed(piece, 2)
+    slot = sums_at
+    waiting = {}
+
+    def advance(group, stage, slot):
+        for piece in range(group * per_half, (group + 1) * per_half):
+            if stage == 0:
+                columns = pl.ds(piece % per_half * sum_width, sum_width)
+                sums = jnp.dot(
+                    hidden_rows[...],
+                    down_w[group, :, columns],
+                    preferred_element_type=jnp.float32,
+                )
+                shape = partial.shape[:3] + (rows, sum_width)
+                partial[:, :, :, :, pl.ds(piece * sum_width, sum_width)] = sums.astype(
+                    jnp.bfloat16
+                ).reshape(shape)
+            else:
+                for copy in waiting[piece]:
+                    copy.wait()
+                add_landed(piece, stage - 1)
+            if stage < 3:
+                waiting[piece], slot = start_sum(piece, stage, slot)
+        return slot
+
+    down_started = forward_weights((2,))
+    for group in range(halves):
+        forwarded((2 + group,), down_started)
+        slot = advance(group, 0, slot)
+        if group + 1 < halves:
+            down_started = forward_weights((3 + group,))
+        if group:
+            slot = advance(group - 1, 2, slot)
+        slot = advance(group, 1, slot)
+        if group:
+            advance(group - 1, 3, slot)
+    slot = advance(halves - 1, 2, slot)
+    advance(halves - 1, 3, slot)
     finish_sends()
 
 
 def whole_layer(sizes, arrays, weights, unit):
-    x, time_step, _, tab, turn, in_map, _, vec, taps, residual, _ = arrays
+    x, time_step, _, in_map, _, _, gain, value_taps, _, residual, _ = arrays
     out_weight, value_weight, gate_weight, down_weight = weights
     span, channels = x.shape
-    groups, lanes = time_step.shape[1], tab.shape[3]
-    chains = turn.shape[1]
+    groups, lanes = time_step.shape[1], 2 * in_map.shape[4]
+    chains = groups
     rows, width = residual.shape
-    pieces = len(gather_paths)
+    pieces, sums_in = len(gather_paths), len(sum_paths)
     count, tp_count = sizes["z"] * sizes["y"], sizes["x"] * sizes["c"]
     grid = tuple(sizes[name] for name in chip_axes)
     blocks = math.prod(grid)
@@ -932,10 +1159,12 @@
             axis = order[stage]
             left = tuple(sizes[name] for name in chip_axes if name not in order[: stage + 1])
             landing.append(
-                pltpu.VMEM((max(sizes[axis] - 1, 1),) + left + (rows, width // pieces), jnp.bfloat16)
+                pltpu.VMEM((max(sizes[axis] - 1, 1),) + left + (rows, width // sums_in), jnp.bfloat16)
             )
-    copies = 2 * pieces * sum(max(sizes[name] - 1, 0) for name in chip_axes)
-    small = max(count, tp_count)
+    gather_hops = pieces * (sizes["y"] + sizes["x"] - 2)
+    sum_hops = sums_in * sum(sizes[name] - 1 for name in chip_axes)
+    deep = sizes["z"] // 2
+    aside = max(per - per // sizes["y"], 1)
     vmem = pl.BlockSpec(memory_space=pltpu.VMEM)
     far = pl.BlockSpec(memory_space=pl.ANY)
     dma = pltpu.SemaphoreType.DMA
@@ -951,32 +1180,43 @@
             pltpu.VMEM((2, span, 3 * groups), bf16),
             pltpu.VMEM((chains, 2, span, lanes), f32),
             pltpu.VMEM((chains, 2, span, lanes), f32),
-            pltpu.VMEM((3 * chains, lanes), f32),
-            pltpu.VMEM((count, 3 * chains, lanes), f32),
+            pltpu.VMEM((chains, 2, 8, lanes), f32),
+            pltpu.VMEM((3, chains, lanes), f32),
+            pltpu.VMEM((chains, lanes), f32),
+            pltpu.VMEM((count, chains, lanes), f32),
+            pltpu.VMEM((2 * chains, lanes), f32),
+            pltpu.VMEM((2 * chains, lanes), bf16),
+            pltpu.VMEM((count, 2 * chains, lanes), bf16),
             pltpu.VMEM((2, chains, lanes), f32),
             pltpu.VMEM((span, channels), f32),
             pltpu.VMEM((tp_count, rows, channels), f32),
-            pltpu.VMEM((tp_count,) + vec.shape, f32),
+            pltpu.VMEM((tp_count,) + gain.shape, f32),
             pltpu.VMEM(out_weight.shape, bf16),
             pltpu.VMEM((rows, width), bf16),
-            pltpu.VMEM((taps.shape[0], unit), f32),
+            pltpu.VMEM((2, value_taps.shape[0], unit), f32),
             pltpu.VMEM((width, 2 * unit), bf16),
-            pltpu.VMEM((unit, width), bf16),
+            pltpu.VMEM((halves, unit, width // halves), bf16),
+            pltpu.VMEM((aside, 2, width // count, unit), bf16),
+            pltpu.VMEM((aside, halves, unit, width // count // halves), bf16),
             pltpu.VMEM(grid + (rows, width), bf16),
             pltpu.VMEM((blocks + 2, rows + 16, 2 * unit), f32),
             pltpu.VMEM((blocks * rows, unit), bf16),
             pltpu.VMEM(grid + (rows, width), bf16),
             *landing,
             dma((1,)),
-            dma((4, small)),
-            dma((4, small)),
-            dma((3,)),
-            dma((copies,)),
-            dma((copies,)),
-            dma((3, per)),
-            dma((3, count)),
-            dma((3, per)),
-            dma((3, per)),
+            dma((tp_count + 2 * count + 2,)),
+            dma((2 * tp_count + 2 * count + 2,)),
+            dma((6,)),
+            dma((gather_hops + sum_hops,)),
+            dma((gather_hops + sum_hops,)),
+            dma((pieces, deep * deep)),
+            dma((pieces, sizes["z"])),
+            dma((2 + halves, aside)),
+            dma((2 + halves, aside)),
+            dma((2 + halves, per)),
+            dma((2 + halves, per)),
+            dma((1 + halves, per)),
+            dma((1 + halves, per)),
         ],
         compiler_params=pltpu.CompilerParams(
             collective_id=2, has_side_effects=True, vmem_limit_bytes=63 * 1024 * 1024
@@ -997,11 +1237,13 @@
     rows, width = residual_shape
     span, states, head = x_shape[0], in_shape[3], in_shape[4]
     fits = (
-        count % sizes["c"] == 0
+        sizes["z"] % 2 == 0
+        and sizes["z"] % sizes["c"] == 0
         and unit % 128 == 0
         and 2 * unit % 256 == 0
         and value_shape[0] % 16 == 0
-        and down_shape[1] % 128 == 0
+        and down_shape[1] % (128 * halves) == 0
+        and width // len(sum_paths) % (down_shape[1] // halves) == 0
         and width % 512 == 0
         and rows % 16 == 0
         and span % 128 == 0
@@ -1032,51 +1274,16 @@
         gate_taps,
         down_weight,
     ) = args
-    span = mixer_input.shape[0]
-    groups, states, head = input_map.shape[2:]
-    pairs = groups // 2
-    number = jnp.arange(states, dtype=jnp.float32)
-
-    def by_pair(array):
-        return array.reshape(2 * pairs, 2 * array.shape[-1])
-
-    near = jnp.arange(1, 9, dtype=jnp.float32)
-    reach = jnp.stack((near, near[::-1]))[:, :, None, None] * number
-    angle = math.pi * turns(time_step[:, None, :, None], reach)
-    tab = jnp.stack((jnp.cos(angle), jnp.sin(angle)))
-    tab = tab.reshape(2, 2, 8, pairs, 2 * states).transpose(1, 3, 0, 2, 4)
-    tab = tab.reshape(2 * pairs, 2, 8, 2 * states)
-    far = math.pi * turns(time_step[:, :, None], number * span)
-    scale = jnp.sqrt(-jnp.expm1(-time_step))
-    total = jnp.exp(-0.5 * span * time_step - jnp.sum(damping, axis=1))
-    turn = jnp.stack(
-        [
-            by_pair(jnp.broadcast_to(item, far.shape))
-            for item in (jnp.cos(far), jnp.sin(far), scale[:, :, None], total[:, :, None])
-        ]
-    )
-    same = jnp.eye(2, dtype=jnp.float32)
-    in_map = input_map.reshape(2, 2, pairs, 2, states, head).transpose(2, 3, 5, 0, 1, 4)
-    in_map = in_map[:, :, :, :, :, None, :] * same[:, None, None, None, :, None].astype(
-        in_map.dtype
-    )
-    in_map = in_map.reshape(pairs, 2 * head, 8 * states)
-    signed = jnp.stack((readout[:, 0], -readout[:, 1]), axis=1)
-    out_map = signed.reshape(2, 2, pairs, 2, head, states).transpose(2, 3, 4, 0, 1, 5)
-    out_map = out_map[:, :, :, :, :, None, :] * same[:, None, None, None, :, None]
-    out_map = out_map.reshape(pairs, 2 * head, 8 * states)
-    vec = jnp.pad(jnp.stack((out_gain, skip_gain)), ((0, 6), (0, 0)))
-    taps = jnp.pad(jnp.concatenate((value_taps, gate_taps)), ((0, 2), (0, 0)))
     arrays = (
         mixer_input,
         time_step,
-        damping,
-        tab,
-        turn,
-        in_map,
-        out_map,
-        vec,
-        taps,
+        damping.swapaxes(1, 2),
+        input_map.swapaxes(3, 4),
+        readout,
+        skip_gain.reshape(1, -1),
+        out_gain.reshape(1, -1),
+        value_taps,
+        gate_taps,
         residual,
         channel_gain.reshape(1, -1),
     )

time: 126 us -> 99.7 us (0.79)
  Pallas kernels: 112 us -> 98 us
  other arithmetic: 6.55 us -> 0 us
  local copies, waits for them, and re-layouts: 7.18 us -> 1.57 us
    pallas_call x1, Pallas kernels: 112 us -> 98 us  [whole_layer(): pl.pallas_call(lambda *refs: layer_kernel(sizes, *refs), name='whole_laye...]
    mul x16 -> x0, local copies, waits for them, and re-layouts: 3.06 us -> none  [the longest x4 1.58 us: one_kernel(): out_map[:, :, :, :, :, None, :] * same[:, None, None, None, :, None]]
    mul x5 -> x0, other arithmetic: 1.75 us -> none  [the longest x1 0.86 us: one_kernel(): out_map[:, :, :, :, :, None, :] * same[:, None, None, None, :, None]]
    transpose x3 -> x0, local copies, waits for them, and re-layouts: 1.36 us -> none  [the longest x1 0.68 us: one_kernel(): tab = tab.reshape(2, 2, 8, pairs, 2 * states).transpose(1, 3, 0, 2, 4)]
where the time goes in v2:
time: 99.7 us; the launch traced here: 99.6 us
  Pallas kernels  98 us (98%)
  local copies, waits for them, and re-layouts  1.57 us (2%)
    pallas_call x1, Pallas kernels, whole_layer(): pl.pallas_call(lambda *refs: layer_kernel(sizes, *refs), name='whole_laye...  98 us

profile of v2, /device:TPU:0, one launch (start us, length us, event | category | flops | bytes accessed | tf_op | source)
XLA Modules:
  0.0 99.6 jit_solution(5255224380197600023)
XLA Ops:
  0.0 98.0 %whole_layer.1 = bf16[32,2048]{1,0:T(8,128)(2,1)} custom-call(bf16[128,256]{1,0:T(8,128)(2,1)} %refs_0_.1, f32[2,16]{1,0:T(2,128)} %refs_1_.1, f32[2,16,128]{2,1,0:T(8,128)} %bitcast.6, bf16[2,2,16,16,64]{4,3,2,1,0:T(8,128)(2,1)} %bitcast.5, f32[2,2,16,16,64]{4,3,2,1,0:T(8,128)} %refs_4_.1, f32[1,256]{1,0:T(1,128)} %bitcast.8, f32[1,256]{1,0:T(1,128)} %bitcast.9, ...), custom_call_target="tpu_custom_call" | custom-call | tf_op jit(solution)/shard_map/whole_layer/pallas_call | solution.py:1172
  98.0 1.6 %copy.17 = bf16[32,2048]{1,0:T(8,128)(2,1)} copy(bf16[32,2048]{1,0:T(8,128)(2,1)} %whole_layer.1) | data formatting | bytes 262144

commit v3 on v2

--- a/solution.py
+++ b/solution.py
@@ -865,7 +865,7 @@
         both = apply(state_high, jnp.concatenate((map_high, map_low), axis=0))
         mixed = both[:, :heads] + both[:, heads:] + apply(state_low, map_high)
         columns = slice(pair * heads, (pair + 1) * heads)
-        y_all[:, columns] = mixed + gains[:, columns]
+        y_all[:, columns] = (mixed + gains[:, columns]).astype(jnp.bfloat16)
     y_copies = []
     for offset in range(1, tp_count):
         peer = lax.rem(tp + offset, tp_count)
@@ -879,6 +879,7 @@
     out_copy.wait()
 
     mixed = jnp.concatenate([y_land[peer] for peer in range(tp_count)], axis=1)
+    mixed = mixed.astype(jnp.float32)
     gain = jnp.concatenate([gain_all[peer] for peer in range(tp_count)], axis=1)
     inverse = lax.rsqrt(jnp.mean(mixed * mixed, axis=1, keepdims=True) + norm_eps)
     normed_mix = (mixed * inverse * gain).astype(jnp.bfloat16)
@@ -945,24 +946,24 @@
     slot = 0
     sums_at = pieces * (sizes["y"] + sizes["x"] - 2)
     pending = [[] for _ in range(pieces)]
-    for stage in range(1, 3):
-        for piece in range(pieces):
-            if stage == 1:
-                line_finish(piece)
-            axis = gather_paths[piece][stage]
-            done = gather_paths[piece][:stage]
-            for copy in pending[piece]:
-                copy.wait()
-            pending[piece] = []
-            index = tuple(slice(None) if name in done else mine[name] for name in chip_axes)
-            block = rows_all.at[index + (slice(None), pl.ds(piece * piece_width, piece_width))]
-            for offset in range(1, sizes[axis]):
-                _, device = neighbour(axis, offset)
-                copy = remote(block, block, hop_send.at[slot], hop_recv.at[slot], device)
-                copy.start()
-                pending[piece].append(copy)
-                slot += 1
+    steps = [(piece + 3 * stage, stage, piece) for stage in (1, 2) for piece in range(pieces)]
+    for _, stage, piece in sorted(steps):
         if stage == 1:
+            line_finish(piece)
+        axis = gather_paths[piece][stage]
+        done = gather_paths[piece][:stage]
+        for copy in pending[piece]:
+            copy.wait()
+        pending[piece] = []
+        index = tuple(slice(None) if name in done else mine[name] for name in chip_axes)
+        block = rows_all.at[index + (slice(None), pl.ds(piece * piece_width, piece_width))]
+        for offset in range(1, sizes[axis]):
+            _, device = neighbour(axis, offset)
+            copy = remote(block, block, hop_send.at[slot], hop_recv.at[slot], device)
+            copy.start()
+            pending[piece].append(copy)
+            slot += 1
+        if stage == 1 and piece == pieces - 1:
             send_weights((0, 1), across)
     for kind in range(2, 2 + halves):
         hand_over((kind,), across)
@@ -995,7 +996,6 @@
 
     lax.fori_loop(0, 2 * unit // chunk, project, 0)
 
-    send_weights((2,), across)
     edges = []
     for kind, (take, land, first) in enumerate(((rows, 0, 1 + core), (8, rows + 8, core))):
         edge = up_rows.at[pl.ds(1, blocks), pl.ds(take, 8), :]
@@ -1003,6 +1003,8 @@
         copy = small(edge, beyond, "edge", kind + 1, partner)
         copy.start()
         edges.append(copy)
+    for kind in range(2, 2 + halves):
+        send_weights((kind,), across)
 
     @pl.when(owns_taps)
     def _():
@@ -1036,8 +1038,6 @@
 
     lax.fori_loop(0, blocks, mix, 0)
 
-    for kind in range(3, 2 + halves):
-        send_weights((kind,), across)
     sum_width = width // sums_in
     per_half = sums_in // halves
 
@@ -1104,13 +1104,13 @@
     slot = sums_at
     waiting = {}
 
-    def advance(group, stage, slot):
-        for piece in range(group * per_half, (group + 1) * per_half):
+    def advance(pair, stage, slot):
+        for piece in range(2 * pair, 2 * pair + 2):
             if stage == 0:
                 columns = pl.ds(piece % per_half * sum_width, sum_width)
                 sums = jnp.dot(
                     hidden_rows[...],
-                    down_w[group, :, columns],
+                    down_w[piece // per_half, :, columns],
                     preferred_element_type=jnp.float32,
                 )
                 shape = partial.shape[:3] + (rows, sum_width)
@@ -1125,19 +1125,20 @@
                 waiting[piece], slot = start_sum(piece, stage, slot)
         return slot
 
+    pair_count = sums_in // 2
+    plan = sorted(
+        (2 * pair + 3 * stage, stage, pair) for pair in range(pair_count) for stage in range(4)
+    )
     down_started = forward_weights((2,))
-    for group in range(halves):
-        forwarded((2 + group,), down_started)
-        slot = advance(group, 0, slot)
-        if group + 1 < halves:
-            down_started = forward_weights((3 + group,))
-        if group:
-            slot = advance(group - 1, 2, slot)
-        slot = advance(group, 1, slot)
-        if group:
-            advance(group - 1, 3, slot)
-    slot = advance(halves - 1, 2, slot)
-    advance(halves - 1, 3, slot)
+    ready = 0
+    for _, stage, pair in plan:
+        group = 2 * pair // per_half
+        if stage == 0 and 2 * pair % per_half == 0:
+            forwarded((2 + group,), down_started)
+            ready = group
+        slot = advance(pair, stage, slot)
+        if stage == 0 and ready + 1 < halves and (2 * pair + 2) % per_half == 0:
+            down_started = forward_weights((3 + ready,))
     finish_sends()
 
 
@@ -1188,8 +1189,8 @@
             pltpu.VMEM((2 * chains, lanes), bf16),
             pltpu.VMEM((count, 2 * chains, lanes), bf16),
             pltpu.VMEM((2, chains, lanes), f32),
-            pltpu.VMEM((span, channels), f32),
-            pltpu.VMEM((tp_count, rows, channels), f32),
+            pltpu.VMEM((span, channels), bf16),
+            pltpu.VMEM((tp_count, rows, channels), bf16),
             pltpu.VMEM((tp_count,) + gain.shape, f32),
             pltpu.VMEM(out_weight.shape, bf16),
             pltpu.VMEM((rows, width), bf16),

time: 99.7 us -> 98.4 us (0.987)
  Pallas kernels: 98 us -> 96.6 us
    pallas_call x1, Pallas kernels: 98 us -> 96.6 us  [whole_layer(): pl.pallas_call(lambda *refs: layer_kernel(sizes, *refs), name='whole_laye...]
where the time goes in v3:
time: 98.4 us; the launch traced here: 98.2 us
  Pallas kernels  96.6 us (98%)
  local copies, waits for them, and re-layouts  1.57 us (2%)
    pallas_call x1, Pallas kernels, whole_layer(): pl.pallas_call(lambda *refs: layer_kernel(sizes, *refs), name='whole_laye...  96.6 us

profile of v3, /device:TPU:0, one launch (start us, length us, event | category | flops | bytes accessed | tf_op | source)
XLA Modules:
  0.0 98.2 jit_solution(5614711191239697113)
XLA Ops:
  0.0 96.6 %whole_layer.1 = bf16[32,2048]{1,0:T(8,128)(2,1)} custom-call(bf16[128,256]{1,0:T(8,128)(2,1)} %refs_0_.1, f32[2,16]{1,0:T(2,128)} %refs_1_.1, f32[2,16,128]{2,1,0:T(8,128)} %bitcast.6, bf16[2,2,16,16,64]{4,3,2,1,0:T(8,128)(2,1)} %bitcast.5, f32[2,2,16,16,64]{4,3,2,1,0:T(8,128)} %refs_4_.1, f32[1,256]{1,0:T(1,128)} %bitcast.8, f32[1,256]{1,0:T(1,128)} %bitcast.9, ...), custom_call_target="tpu_custom_call" | custom-call | tf_op jit(solution)/shard_map/whole_layer/pallas_call | solution.py:1173
  96.6 1.6 %copy.17 = bf16[32,2048]{1,0:T(8,128)(2,1)} copy(bf16[32,2048]{1,0:T(8,128)(2,1)} %whole_layer.1) | data formatting | bytes 262144
